TPU v7x, 512 devices: a whole 4x4x16 slice. The times are simulated.
512 devices in a mesh: sp: 64 (over z, y), tp: 8 (over x, core).
Axes of the slice: x: 4, y: 4, z: 16, core: 2. Of those that a mesh axis runs over, the one named last changes fastest.
Arguments:
- tokens: bfloat16 [8192, 2048], P(('sp', 'tp')), may hold values from -6 to 6
- input_norm_gain: float32 [2048], replicated, may hold values from 0.1 to 1.9
- differential_query: bfloat16 [2048, 1024], P(None, 'tp'), may hold values from -0.176776695 to 0.176776695, as said below
- differential_key: bfloat16 [2048, 1024], P(None, 'tp'), may hold values from -0.176776695 to 0.176776695, as said below
- differential_value: bfloat16 [2048, 1024], P(None, 'tp'), may hold values from -0.125 to 0.125
- query_norm_gain: float32 [64], replicated, may hold values from 1.15 to 5
- key_norm_gain: float32 [64], replicated, may hold values from 1.15 to 5
- second_map_weight: float32 [8], P('tp'), may hold values from 0.3 to 0.8
- differential_norm_gain: float32 [128], replicated, may hold values from 0.1 to 1.9
- linear_query: bfloat16 [2048, 512], P(None, 'tp'), may hold values from -0.125 to 0.125
- linear_key: bfloat16 [2048, 512], P(None, 'tp'), may hold values from -0.125 to 0.125
- linear_value: bfloat16 [2048, 1024], P(None, 'tp'), may hold values from -0.125 to 0.125
- linear_output_gate: bfloat16 [2048, 1024], P(None, 'tp'), may hold values from -0.125 to 0.125
- forget_down_factor: bfloat16 [2048, 32], replicated, may hold values from -0.125 to 0.125
- forget_up_factor: bfloat16 [32, 512], P(None, 'tp'), may hold values from -2.109375 to 2.109375
- forget_bias: float32 [512], P('tp'), may hold values from -0.5 to 10
- extra_shrinkage_exponent: float32 [8192, 8], P('sp', 'tp'), may hold values from -1.5 to 0
- linear_norm_gain: float32 [128], replicated, may hold values from 0.1 to 1.9
- differential_output_rows: bfloat16 [1024, 2048], P('tp'), may hold values from -0.125 to 0.125
- linear_output_rows: bfloat16 [1024, 2048], P('tp'), may hold values from -0.125 to 0.125
Outputs:
- layer_out: bfloat16 [8192, 2048], P(('sp', 'tp'))
Inputs may be any that keep to these rules, and one draw needn't show every extreme that they name: `differential_query`: independent entries of scale one over sqrt(2048). `differential_key`: entries of scale one over sqrt(2048).
All inputs are finite; a program needn't handle non-finite values.
Results may differ from a plain program's by a relative error of at most 0.015.
Values may be sent and summed in bfloat16 or wider, within the bound.
No kernel may reach another device: no remote copies, remote signals or barrier semaphores. Data moves between devices by JAX's collectives and lax.ppermute only.
A program may use at most 64 MiB of HBM per device.

v0:
```python
from functools import partial

import jax
import jax.numpy as jnp
from jax import lax
from jax.sharding import Mesh
from jax.sharding import PartitionSpec as P

HEAD = 64
VDIM = 128
RECURRENT_DIM = 64
GLA_DV = 128
BLOCK = 64
SP = ("sp_0", "sp_1")
SP_TP = ("sp_0", "sp_1", "tp")


RMS_EPS = 1e-06
SOFTMAX_DIVISOR = 16.0
OUT_SCALE = 0.8
NEG_LARGE = -1e30


def sent_to_all(shard, axis):
    copies = jnp.broadcast_to(shard, (lax.axis_size(axis), *shard.shape))
    return lax.all_to_all(copies, axis, split_axis=0, concat_axis=0, tiled=True)


def laid_out(blocks, dim):
    blocks = jnp.moveaxis(blocks, 0, dim)
    lengths = blocks.shape
    return blocks.reshape(*lengths[:dim], lengths[dim] * lengths[dim + 1], *lengths[dim + 2 :])


def gathered_copies(shard, axis, dim):
    blocks = sent_to_all(shard, axis)
    return laid_out(blocks, dim)


def side_by_side(arrays, axis, dim, along):
    both = jnp.concatenate(arrays, axis=along)
    whole, at, outs = (lax.all_gather(both, axis, axis=dim, tiled=True), 0, [])
    for a in arrays:
        outs.append(lax.slice_in_dim(whole, at, at + a.shape[along], axis=along))
        at += a.shape[along]
    return tuple(outs)


def nothing_yet(shard, identity):
    return jax.tree.map(
        lambda part, zero: jnp.zeros_like(part) + jnp.asarray(zero, part.dtype), shard, identity
    )


def all_in_one(shard, axis):
    leaves = jax.tree.leaves(shard)
    sequence = sorted(range(len(leaves)), key=lambda k: -leaves[k].size)
    width = (1, *leaves[sequence[0]].shape)[-1]
    lines = [
        jnp.pad(leaves[k].reshape(-1), (0, -leaves[k].size % width)).reshape(-1, width)
        for k in sequence
    ]
    both, at, found = (lax.all_gather(jnp.concatenate(lines), axis), 0, {})
    for k, line in zip(sequence, lines):
        section = both[:, at : at + len(line)].reshape(len(both), -1)
        found[k] = section[:, : leaves[k].size].reshape(-1, *leaves[k].shape)
        at += len(line)
    numbers = iter(range(len(leaves)))
    return jax.tree.map(lambda _: found[next(numbers)], shard)


def prefix_by_axis(shard, axes, combine, identity):
    before = start = nothing_yet(shard, identity)
    so_far = shard
    for axis in reversed(axes):
        devices, position = (lax.axis_size(axis), lax.axis_index(axis))
        pieces = all_in_one(so_far, axis)
        inside, so_far = (start, start)
        for k in range(devices):
            passed = k < position
            so_far = combine(so_far, jax.tree.map(lambda part: part[k], pieces))
            inside = jax.tree.map(lambda new, old: jnp.where(passed, new, old), so_far, inside)
        before = combine(inside, before)
    return before


def split_up(shard, dim, devices):
    lengths = shard.shape
    blocks = shard.reshape(*lengths[:dim], devices, lengths[dim] // devices, *lengths[dim + 1 :])
    return jnp.moveaxis(blocks, dim, 0)


def summed_on_arrival(shard, axis, dim):
    blocks = split_up(shard, dim, lax.axis_size(axis))
    arrived = lax.all_to_all(blocks, axis, split_axis=0, concat_axis=0, tiled=True)
    return arrived.astype(jnp.float32).sum(axis=0)


def rms_scale(values, scale_gain):
    mean_sq = jnp.mean(values * values, axis=-1, keepdims=True)
    return values * lax.rsqrt(mean_sq + RMS_EPS) * scale_gain


def block_length(total_rows, shard_rows):
    best = shard_rows
    shard_total = total_rows // shard_rows
    for multiple in range(1, shard_total + 1):
        if shard_total % multiple == 0 and shard_rows * multiple <= 2048:
            best = shard_rows * multiple
    return best


def combine_chain(earlier, later):
    return (earlier[0] * later[0], earlier[1] * later[0][..., None] + later[1])


def keep_carry(carry_now):
    return carry_now


def attend_span(query_set, query_pos, keys_here, values_here, key_pos, carry_now):
    row_peaks, totals, numerators = carry_now
    query_rows = query_set.shape[0]
    group_count = query_set.shape[1]
    attn_heads = group_count // 2
    span_rows = keys_here.shape[0]
    scores = jnp.einsum(
        "tgd,kgd->gtk", query_set, keys_here, preferred_element_type=jnp.float32
    ) * HEAD ** (-0.5)
    causal = key_pos[None, :] <= query_pos[:, None]
    scores = jnp.where(causal[None], scores, NEG_LARGE)
    new_peaks = jnp.maximum(row_peaks, jnp.max(scores, axis=-1))
    weights = jnp.where(causal[None], jnp.exp(scores - new_peaks[..., None]), 0.0)
    factor = jnp.exp(row_peaks - new_peaks)
    totals = totals * factor + jnp.sum(weights, axis=-1)
    rounded = weights.astype(jnp.bfloat16).reshape(attn_heads, 2, query_rows, span_rows)
    contrib = jnp.einsum(
        "hmtk,khv->hmtv", rounded, values_here, preferred_element_type=jnp.float32
    ).reshape(group_count, query_rows, VDIM)
    return (new_peaks, totals, numerators * factor[..., None] + contrib)


def per_device(
    tokens,
    input_norm_gain,
    differential_query,
    differential_key,
    differential_value,
    query_norm_gain,
    key_norm_gain,
    second_map_weight,
    differential_norm_gain,
    linear_query,
    linear_key,
    linear_value,
    linear_output_gate,
    forget_down_factor,
    forget_up_factor,
    forget_bias,
    extra_shrinkage_exponent,
    linear_norm_gain,
    differential_output_rows,
    linear_output_rows,
):
    sp_index = lax.axis_index(SP)
    attn_heads = second_map_weight.shape[0]
    linear_head_list = extra_shrinkage_exponent.shape[1]
    normed = rms_scale(tokens.astype(jnp.float32), input_norm_gain).astype(jnp.bfloat16)
    parts_list = [
        differential_query,
        differential_key,
        differential_value,
        linear_query,
        linear_key,
        linear_value,
        linear_output_gate,
        forget_down_factor,
    ]
    packed = jnp.concatenate(parts_list, axis=1)
    bounds = [0]
    for matrix in parts_list:
        bounds.append(bounds[-1] + matrix.shape[1])
    projected = jnp.dot(
        gathered_copies(normed, "tp", 0), packed, preferred_element_type=jnp.float32
    ).astype(jnp.bfloat16)
    row_count = projected.shape[0]

    def section(column_set):
        return projected[:, bounds[column_set] : bounds[column_set + 1]]

    group_count = 2 * attn_heads
    query_norm = rms_scale(
        section(0).astype(jnp.float32).reshape(row_count, group_count, HEAD), query_norm_gain
    ).astype(jnp.bfloat16)
    key_norm = rms_scale(
        section(1).astype(jnp.float32).reshape(row_count, group_count, HEAD), key_norm_gain
    ).astype(jnp.bfloat16)
    key_flat = key_norm.reshape(row_count, group_count * HEAD)
    value_flat = section(2)
    full_pos = sp_index * row_count + jnp.arange(row_count, dtype=jnp.int32)
    query_sets = [(query_norm, full_pos)]
    fold_start = tuple(
        (
            (
                jnp.full((group_count, query_set.shape[0]), NEG_LARGE, jnp.float32),
                jnp.zeros((group_count, query_set.shape[0]), jnp.float32),
                jnp.zeros((group_count, query_set.shape[0], VDIM), jnp.float32),
            )
            for query_set, query_pos in query_sets
        )
    )
    key_rows, value_rows = side_by_side((key_flat, value_flat), SP, 0, 1)
    piece_rows = key_rows.shape[0]
    span_rows = block_length(piece_rows, row_count)

    def attend(span_index, carries):
        row_start = span_index * span_rows
        keys_here = lax.dynamic_slice_in_dim(
            key_rows, span_index * span_rows, span_rows, 0
        ).reshape(span_rows, group_count, HEAD)
        values_here = lax.dynamic_slice_in_dim(
            value_rows, span_index * span_rows, span_rows, 0
        ).reshape(span_rows, attn_heads, VDIM)
        key_pos = row_start + jnp.arange(span_rows, dtype=jnp.int32)
        results = []
        for (query_set, query_pos), carry_in in zip(query_sets, carries):
            work = partial(attend_span, query_set, query_pos, keys_here, values_here, key_pos)
            results.append(lax.cond(row_start <= jnp.max(query_pos), work, keep_carry, carry_in))
        return tuple(results)

    folded = lax.fori_loop(0, piece_rows // span_rows, attend, fold_start)
    row_peaks, totals, numerators = folded[0]
    set_rows = totals.shape[1]
    maps_out = (numerators / totals[..., None]).reshape(attn_heads, 2, set_rows, VDIM)
    attn_mix = maps_out[:, 0] - second_map_weight[:, None, None] * maps_out[:, 1]
    attn_out = (
        (rms_scale(attn_mix, differential_norm_gain) * OUT_SCALE)
        .transpose(1, 0, 2)
        .reshape(set_rows, attn_heads * VDIM)
        .astype(jnp.bfloat16)
    )
    chain_queries = section(3).astype(jnp.float32).reshape(
        row_count, linear_head_list, RECURRENT_DIM
    ) * RECURRENT_DIM ** (-0.5)
    chain_keys = section(4).astype(jnp.float32).reshape(row_count, linear_head_list, RECURRENT_DIM)
    chain_values = section(5).astype(jnp.float32).reshape(row_count, linear_head_list, GLA_DV)
    gated = jax.nn.silu(section(6).astype(jnp.float32)).reshape(row_count, linear_head_list, GLA_DV)
    sigmoid_preactivation = (
        jnp.dot(section(7), forget_up_factor, preferred_element_type=jnp.float32) + forget_bias
    )
    shrinkage_exponent = (
        jax.nn.log_sigmoid(sigmoid_preactivation).reshape(
            row_count, linear_head_list, RECURRENT_DIM
        )
        / SOFTMAX_DIVISOR
        + extra_shrinkage_exponent[:, :, None]
    )
    block_total = row_count // BLOCK

    def blockify(array):
        return array.reshape(block_total, BLOCK, linear_head_list, array.shape[-1])

    causal_block = jnp.arange(BLOCK)[:, None] >= jnp.arange(BLOCK)[None, :]

    def chain_block(carry, inputs):
        carried, log_total = carry
        query_block, key_block, value_block, decay_block = inputs
        log_cum = jnp.cumsum(decay_block, axis=0)
        log_last = log_cum[-1]
        query_decayed = query_block * jnp.exp(log_cum)
        key_inverse = key_block * jnp.exp(-log_cum)
        inner_scores = jnp.einsum("thd,shd->hts", query_decayed, key_inverse)
        inner_scores = jnp.where(causal_block[None], inner_scores, 0.0)
        local_out = jnp.einsum("hts,she->the", inner_scores, value_block)
        local_out = local_out + jnp.einsum("thd,hde->the", query_decayed, carried)
        key_end = key_block * jnp.exp(log_last[None] - log_cum)
        carried = carried * jnp.exp(log_last)[..., None] + jnp.einsum(
            "thd,the->hde", key_end, value_block
        )
        carried_query = query_decayed * jnp.exp(log_total)[None]
        return ((carried, log_total + log_last), (local_out, carried_query))

    chain_zero = (
        jnp.zeros((linear_head_list, RECURRENT_DIM, GLA_DV), jnp.float32),
        jnp.zeros((linear_head_list, RECURRENT_DIM), jnp.float32),
    )
    (own_state, log_total), (local_out, carried_query) = lax.scan(
        chain_block,
        chain_zero,
        (
            blockify(chain_queries),
            blockify(chain_keys),
            blockify(chain_values),
            blockify(shrinkage_exponent),
        ),
    )
    local_out = local_out.reshape(row_count, linear_head_list, GLA_DV)
    carried_query = carried_query.reshape(row_count, linear_head_list, RECURRENT_DIM)
    own_decay = jnp.exp(log_total)
    carried_in = prefix_by_axis(
        (own_decay, own_state),
        SP,
        combine_chain,
        (jnp.ones_like(own_decay), jnp.zeros_like(own_state)),
    )[1]
    chain_full = local_out + jnp.einsum("thd,hde->the", carried_query, carried_in)
    chain_out = (
        (rms_scale(chain_full, linear_norm_gain) * gated)
        .reshape(row_count, linear_head_list * GLA_DV)
        .astype(jnp.bfloat16)
    )
    mixed_out = summed_on_arrival(
        (
            jnp.dot(attn_out, differential_output_rows, preferred_element_type=jnp.float32)
            + jnp.dot(chain_out, linear_output_rows, preferred_element_type=jnp.float32)
        ).astype(jnp.bfloat16),
        "tp",
        0,
    )
    return mixed_out.astype(jnp.bfloat16)


def solution(mesh):
    torus = Mesh(mesh.devices.reshape(16, 4, mesh.shape["tp"]), ("sp_0", "sp_1", "tp"))
    placed = (
        P(SP_TP, None),
        P(),
        P(None, "tp"),
        P(None, "tp"),
        P(None, "tp"),
        P(),
        P(),
        P("tp"),
        P(),
        P(None, "tp"),
        P(None, "tp"),
        P(None, "tp"),
        P(None, "tp"),
        P(),
        P(None, "tp"),
        P("tp"),
        P(SP, "tp"),
        P(),
        P("tp", None),
        P("tp", None),
    )
    return jax.shard_map(
        per_device, mesh=torus, in_specs=placed, out_specs=P(SP_TP, None), check_vma=False
    )
```

profile of v0, /device:TPU:1, one launch (start us, length us, event | category | flops | bytes accessed | tf_op | source)
XLA Modules:
  0.0 215.2 jit_solution(5521990056743395399)
XLA Ops:
  6.5 0.0 copy-start
  6.5 1.1 fusion.55
  7.6 0.9 fusion.57
  8.6 0.9 broadcast_in_dim.91
  9.4 10.2 %all-to-all-start = ((bf16[8,16,2048]{2,1,0:T(8,128)(2,1)}), bf16[8,16,2048]{2,1,0:T(8,128)(2,1)S(1)}, u32[]{:S(2)}, u32[]{:S(2)}) async-start(bf16[8,16,2048]{2,1,0:T(8,128)(2,1)} %broadcast_in_dim.91), calls=%async_computation | async-start | bytes 1048576 | tf_op jit(solution)/shard_map/all_to_all | solution.py:26
  19.7 0.0 all-gather.6.cloned.1.call-start
  19.7 1.2 copy.45
  20.9 0.0 copy-done.3
  20.9 0.3 copy.46
  21.2 0.0 copy-done.4
  21.2 0.3 copy.47
  21.5 0.0 copy-done.9
  21.5 0.1 mul.486
  21.6 0.0 copy-done.2
  21.6 6.2 %concatenate.12 = bf16[2048,800]{1,0:T(8,128)(2,1)} concatenate(bf16[2048,128]{1,0:T(8,128)(2,1)S(1)} %copy-done.2, bf16[2048,128]{1,0:T(8,128)(2,1)} %param.29, bf16[2048,128]{1,0:T(8,128)(2,1)} %param.30, bf16[2048,64]{1,0:T(8,128)(2,1)S(1)} %copy.45, bf16[2048,64]{1,0:T(8,128)(2,1)S(1)} %copy.46, bf16[2048,128]{1,0:T(8,128)(2,1)} %param.37, bf16[2048,128]{1,0:T(8,128)(2,1)} %param.38, ...), dimensions={1} | concatenate | bytes 6553600 | tf_op jit(solution)/shard_map/concatenate | solution.py:179
  27.8 1.2 all-to-all-done
  29.0 3.6 %convolution_convert_fusion = bf16[128,800]{0,1:T(8,128)(2,1)S(1)} fusion(bf16[128,2048]{1,0:T(8,128)(2,1)S(1)} %bitcast.228, bf16[2048,800]{1,0:T(8,128)(2,1)} %concatenate.12), kind=kOutput, calls=%fused_computation.65 | convolution fusion | flops 419532800 | bytes 4005888 | tf_op jit(solution)/shard_map/dot_general | solution.py:183
  32.7 0.1 fusion.59
  32.8 0.6 pad_maximum_fusion
  33.4 0.0 all-gather.6.cloned.1.call-update
  33.5 0.6 add_reduce_fusion
  34.8 0.1 copy.49
  34.9 0.0 copy-done.8
  34.9 0.0 copy-done.10
  34.9 0.0 copy-done.11
  34.9 0.2 fusion.79
  35.1 0.1 copy.57
  35.3 0.1 copy.58
  35.4 0.1 copy.59
  35.5 1.5 while.37
  35.5 0.1 fusion.210
  35.6 0.3 fusion.213
  35.8 0.1 fusion.214
  36.0 0.2 fusion.212
  36.3 0.1 fusion.210
  36.3 0.3 fusion.213
  36.6 0.1 fusion.214
  36.7 0.2 fusion.212
  37.0 0.0 copy-start.5
  37.0 9.1 %all-gather.2 = f32[4,65,128]{2,1,0:T(8,128)S(1)} all-gather(f32[1,65,128]{2,1,0:T(8,128)S(1)} %maximum_bitcast_fusion), channel_id=2, replica_groups=mesh['sp_0'=16,'sp_1'=4,'tp'=8] {'sp_1'}, dimensions={0}, use_global_device_ids=true | all-gather | bytes 166400 | tf_op jit(solution)/shard_map/all_gather | solution.py:63
  46.2 0.1 fusion.188
  46.3 29.9 %all-gather.3 = f32[16,65,128]{2,1,0:T(8,128)S(1)} all-gather(f32[1,65,128]{2,1,0:T(8,128)S(1)} %maximum_bitcast_fusion.1), channel_id=3, replica_groups=mesh['sp_0'=16,'sp_1'=4,'tp'=8] {'sp_0'}, dimensions={0}, use_global_device_ids=true | all-gather | bytes 565760 | tf_op jit(solution)/shard_map/all_gather | solution.py:63
  76.2 0.1 copy.55
  76.4 0.5 multiply_reduce_fusion
  76.9 0.1 fusion.68
  77.0 91.8 %all-gather.6.cloned.1.call-done = bf16[8192,256]{0,1:T(8,128)(2,1)} async-done(((bf16[128,256]{0,1:T(8,128)(2,1)}), bf16[8192,256]{0,1:T(8,128)(2,1)}) %all-gather.6.cloned.1.call-update) | async-done | bytes 4194320 | tf_op jit(solution)/shard_map/all_gather | solution.py:42
  168.8 3.9 %fusion.175 = (bf16[8192,128]{0,1:T(8,128)(2,1)}, bf16[8192,128]{0,1:T(8,128)(2,1)S(1)}) fusion(bf16[8192,256]{0,1:T(8,128)(2,1)} %all-gather.6.cloned.1.call-done), kind=kLoop, calls=%fused_computation.263 | loop fusion | bytes 8388608 | tf_op jit(solution)/shard_map/slice | solution.py:44
  172.7 4.1 %copy.48 = bf16[8192,128]{1,0:T(8,128)(2,1)} copy(bf16[8192,128]{0,1:T(8,128)(2,1)} %get-tuple-element.531) | data formatting | bytes 4194304
  176.8 0.0 copy-start.6
  176.8 0.0 copy-start.7
  176.8 5.8 %while.36 = (s32[]{:T(128)}, f32[2,128]{1,0:T(2,128)S(1)}, f32[2,128]{1,0:T(2,128)S(1)}, f32[2,128,128]{2,1,0:T(8,128)S(1)}, s32[]{:T(128)}, /*index=5*/bf16[819...) while((s32[]{:T(128)}, f32[2,128]{1,0:T(2,128)S(1)}, ...), condition=%wide.region_9.10_spmd.clone, body=%wide.region_4.9_spmd.clone.sunk | while | flops 206375552 | bytes 9783617 | solution.py:231
  177.5 3.3 %conditional.3 = ((f32[2,128]{1,0:T(2,128)S(1)}, f32[2,128]{1,0:T(2,128)S(1)}, f32[2,128,128]{2,1,0:T(8,128)S(1)})) conditional(s32[]{:T(128)} %convert_element_type.122, (f32[2,128]{1,0:T(2,128)S(1)}, f32[2,128]{1,0:T(2,128)S(1)}, f32[2,128,128]{2,1,0:T(8,128)S(1)}) %tuple.105, (s32[]{:T(128)}, s32[2048]{0:T(1024)S(1)}, s32[]{:T(128)}, ...), branch_computations={%region_5.0_spmd, %region_6.8_spmd} | conditional | flops 206375552 | bytes 9774674 | solution.py:228
  177.6 0.3 broadcast_compare_fusion
  177.9 0.6 fusion.174
  178.6 0.4 fusion.7
  179.0 1.8 convolution_add_fusion
  182.7 0.0 copy-start.1
  182.7 0.1 divide_bitcast_fusion
  182.8 0.1 multiply_reduce_fusion.1
  182.9 0.3 fusion.73
  183.3 0.4 copy-done.1
  183.7 0.4 fusion.52
  184.1 23.5 %all_to_all.10 = bf16[8,16,2048]{2,1,0:T(8,128)(2,1)S(1)} all-to-all(bf16[8,16,2048]{2,1,0:T(8,128)(2,1)S(1)} %bitcast.229), channel_id=1, replica_groups=mesh['sp_0'=16,'sp_1'=4,'tp'=8] {'tp'}, dimensions={0} | all-to-all | bytes 1048576 | tf_op jit(solution)/shard_map/all_to_all | solution.py:95
  207.6 0.7 reduce_sum.74
  (67 shorter events, 0.4 us)
Async XLA Ops:
  6.5 176.4 %copy-start = (bf16[128,2048]{1,0:T(8,128)(2,1)S(1)}, bf16[128,2048]{1,0:T(8,128)(2,1)}, u32[]{:S(2)}) copy-start(bf16[128,2048]{1,0:T(8,128)(2,1)} %param.44) | copy-start | bytes 1572868
  6.5 14.3 %copy-start.3 = (bf16[2048,64]{0,1:T(8,128)(2,1)S(1)}, bf16[2048,64]{0,1:T(8,128)(2,1)}, u32[]{:S(2)}) copy-start(bf16[2048,64]{0,1:T(8,128)(2,1)} %param.36) | copy-start | bytes 786436
  6.5 14.6 %copy-start.4 = (bf16[2048,32]{0,1:T(8,128)(2,1)S(1)}, bf16[2048,32]{0,1:T(8,128)(2,1)}, u32[]{:S(2)}) copy-start(bf16[2048,32]{0,1:T(8,128)(2,1)} %param.39) | copy-start | bytes 393220
  6.5 14.9 %copy-start.9 = (f32[64]{0:T(128)S(1)}, f32[64]{0:T(128)}, u32[]{:S(2)}) copy-start(f32[64]{0:T(128)} %param.32) | copy-start | bytes 772
  6.5 15.0 %copy-start.2 = (bf16[2048,128]{1,0:T(8,128)(2,1)S(1)}, bf16[2048,128]{1,0:T(8,128)(2,1)}, u32[]{:S(2)}) copy-start(bf16[2048,128]{1,0:T(8,128)(2,1)} %param.28) | copy-start | bytes 1572868
  9.4 19.6 %all-to-all-start = ((bf16[8,16,2048]{2,1,0:T(8,128)(2,1)}), bf16[8,16,2048]{2,1,0:T(8,128)(2,1)S(1)}, u32[]{:S(2)}, u32[]{:S(2)}) async-start(bf16[8,16,2048]{2,1,0:T(8,128)(2,1)} %broadcast_in_dim.91), calls=%async_computation | async-start | bytes 1048576 | tf_op jit(solution)/shard_map/all_to_all | solution.py:26
  19.7 149.1 %all-gather.6.cloned.1.call-start = ((), (), s32[]{:S(2)}) async-start(), calls=%async_computation.2 | async-start | bytes 4259840 | tf_op jit(solution)/shard_map/all_gather | solution.py:42
  29.0 5.9 %copy-start.8 = (bf16[32,64]{1,0:T(8,128)(2,1)S(1)}, bf16[32,64]{1,0:T(8,128)(2,1)}, u32[]{:S(2)}) copy-start(bf16[32,64]{1,0:T(8,128)(2,1)} %param.40) | copy-start | bytes 12292
  29.0 5.9 %copy-start.10 = (f32[128,1]{0,1:T(1,128)S(1)}, f32[128,1]{0,1:T(1,128)}, u32[]{:S(2)}) copy-start(f32[128,1]{0,1:T(1,128)} %param.42) | copy-start | bytes 1540
  29.0 5.9 %copy-start.11 = (f32[64]{0:T(128)S(1)}, f32[64]{0:T(128)}, u32[]{:S(2)}) copy-start(f32[64]{0:T(128)} %param.41) | copy-start | bytes 772
  37.0 39.9 %copy-start.5 = (f32[64]{0:T(128)S(1)}, f32[64]{0:T(128)}, u32[]{:S(2)}) copy-start(f32[64]{0:T(128)} %param.31) | copy-start | bytes 772
  176.8 6.1 %copy-start.6 = (f32[128]{0:T(128)S(1)}, f32[128]{0:T(128)}, u32[]{:S(2)}) copy-start(f32[128]{0:T(128)} %param.34) | copy-start | bytes 1540
  176.8 6.4 %copy-start.7 = (f32[128]{0:T(128)S(1)}, f32[128]{0:T(128)}, u32[]{:S(2)}) copy-start(f32[128]{0:T(128)} %param.43) | copy-start | bytes 1540
  182.7 1.0 copy-start.1
Sparse Core Ops, SparseCore 0:
  33.6 135.1 all-gather.5
where the time goes:
time: 218 us; the launch traced here: 215 us
  waiting for transfers between devices  93.1 us (43%)
  blocking collectives  62.6 us (29%)
  local copies, waits for them, and re-layouts  18 us (8%)
  between operations  14.5 us (7%)
  starting transfers between devices  10.2 us (5%)
  matrix products  8.6 us (4%)
  other arithmetic  5.59 us (3%)
  loops' own time  2.63 us (1%)
    all_gather x1, waiting for transfers between devices, side_by_side(): whole, at, outs = (lax.all_gather(both, axis, axis=dim, tiled=True), 0, [])  91.8 us
    all_gather x2, blocking collectives, all_in_one(): both, at, found = (lax.all_gather(jnp.concatenate(lines), axis), 0, {})  39 us
    all_to_all x1, blocking collectives, summed_on_arrival(): lax.all_to_all(blocks, axis, split_axis=0, concat_axis=0, tiled=True)  23.5 us
    all_to_all x1, starting transfers between devices, sent_to_all(): return lax.all_to_all(copies, axis, split_axis=0, concat_axis=0, tiled=True)  10.2 us
    unnamed x31, local copies, waits for them, and re-layouts  6.6 us
    concatenate x1, local copies, waits for them, and re-layouts, per_device(): packed = jnp.concatenate(parts_list, axis=1)  6.22 us
  transfers between devices with their start and end apart: 2, of which 2 were waited for; matrix products, arithmetic and copies ran while one was open for 5% of the time, Pallas kernels for 0%

commit v1 on v0

v1 whole, which is shorter than its diff:
```python
import jax
import jax.numpy as jnp
from jax import lax
from jax.experimental import pallas as pl
from jax.experimental.pallas import tpu as pltpu
from jax.sharding import Mesh
from jax.sharding import PartitionSpec as P

F32 = jnp.float32
BF16 = jnp.bfloat16
HEAD = 64
VDIM = 128
BLOCK = 128
SUB = 16
GROUPS = 8
MEMBERS = 8
SP = ("far", "pair", "y")
TEAM = ("pair", "y")
SP_TP = ("far", "pair", "y", "tp")
RMS_EPS = 1e-06
NEG_LARGE = -1e30
NT = (((1,), (1,)), ((), ()))


def two_parts(x):
    high = x.astype(BF16).astype(F32)
    return high, (x - high).astype(BF16).astype(F32)


def three_parts(x):
    high, rest = x.astype(BF16).astype(F32), None
    middle = (x - high).astype(BF16).astype(F32)
    rest = ((x - high) - middle).astype(BF16).astype(F32)
    return high, middle, rest


def dot(a, b):
    return jnp.dot(a, b, preferred_element_type=F32)


def dot_nt(a, b):
    return lax.dot_general(a, b, NT, preferred_element_type=F32)


def iota(shape, dim):
    return lax.broadcasted_iota(jnp.int32, shape, dim)


def two_map_norm(values, gain):
    first = iota(values.shape, 1) < HEAD
    squares = values * values
    low = jnp.sum(jnp.where(first, squares, 0.0), axis=1, keepdims=True)
    high = jnp.sum(jnp.where(first, 0.0, squares), axis=1, keepdims=True)
    mean_sq = jnp.where(first, low, high) * (1.0 / HEAD)
    return values * lax.rsqrt(mean_sq + RMS_EPS) * jnp.concatenate([gain, gain], axis=1)


def project_kernel(
    rows_ref, gain_ref, dq_ref, dk_ref, dv_ref, lq_ref, lk_ref, lv_ref, lg_ref, down_ref, up_ref,
    bias_ref, shrink_ref, qgain_ref, kgain_ref,
    team_ref, kv_ref, local_ref, decayed_ref, gate_ref, scores_ref,
):
    rows = rows_ref[...].reshape(BLOCK, rows_ref.shape[-1]).astype(F32)
    mean_sq = jnp.mean(rows * rows, axis=1, keepdims=True)
    normed = (rows * lax.rsqrt(mean_sq + RMS_EPS) * gain_ref[...]).astype(BF16)

    def project(ref):
        return dot(normed, ref[...]).astype(BF16)

    query = two_map_norm(project(dq_ref).astype(F32), qgain_ref[...]).astype(BF16)
    query = query * jnp.asarray(HEAD**-0.5, BF16)
    key = two_map_norm(project(dk_ref).astype(F32), kgain_ref[...]).astype(BF16)
    kv_ref[0:BLOCK] = key
    kv_ref[BLOCK:] = project(dv_ref)
    gate = project(lg_ref).astype(F32)
    gate_ref[...] = gate * jax.nn.sigmoid(gate)

    low = project(down_ref)
    pre = dot(low, up_ref[...]) + bias_ref[...]
    log_sig = jnp.minimum(pre, 0.0) - jnp.log1p(jnp.exp(-jnp.abs(pre)))
    log_a = log_sig * (1.0 / 16.0) + shrink_ref[...]
    lower = (iota((BLOCK, BLOCK), 0) >= iota((BLOCK, BLOCK), 1)).astype(BF16)
    total = sum(dot(lower, part.astype(BF16)) for part in three_parts(log_a))

    lq = project(lq_ref).astype(F32) * HEAD**-0.5
    lk = project(lk_ref).astype(F32)
    lv = project(lv_ref)
    scores_ref[...] = jnp.zeros_like(scores_ref)
    for step in range(1, BLOCK // SUB):
        at = step * SUB
        border = total[at - 1 : at]
        q_part = lq[at : at + SUB] * jnp.exp(total[at : at + SUB] - border)
        k_part = lk[:at] * jnp.exp(border - total[:at])
        scores_ref[at : at + SUB, 0:at] = dot_nt(q_part.astype(BF16), k_part.astype(BF16))
    scores = scores_ref[...]
    row = iota((BLOCK, BLOCK), 0)
    distance = row - iota((BLOCK, BLOCK), 1)
    for shift in range(SUB):
        k_part = lk if shift == 0 else pltpu.roll(lk, shift, 0)
        if shift == 0:
            terms = lq * k_part
        else:
            terms = lq * k_part * jnp.exp(jnp.minimum(total - pltpu.roll(total, shift, 0), 0.0))
        column = jnp.sum(terms, axis=1, keepdims=True)
        here = (distance == shift) & (row % SUB >= shift)
        scores = jnp.where(here, column, scores)
    local_ref[...] = dot(scores.astype(BF16), lv)
    decayed_ref[...] = (lq * jnp.exp(total)).astype(BF16)

    k_end = lk * jnp.exp(total[BLOCK - 1 :] - total)
    flipped = jnp.concatenate([total, k_end], axis=1).T
    decay = jnp.broadcast_to(flipped[:HEAD, BLOCK - 1 :], (HEAD, VDIM))
    state = dot(flipped[HEAD:].astype(BF16), lv)
    state_parts = two_parts(state)
    decay_parts = two_parts(decay)
    for member in range(MEMBERS):
        own = slice(member * 8, member * 8 + 8)
        team_ref[member, 0:BLOCK] = query
        team_ref[member, BLOCK:] = jnp.concatenate(
            [part[own] for part in (*state_parts, *decay_parts)], axis=0
        ).astype(BF16)


def joined(block, at):
    return block[at : at + 8] + block[at + 8 : at + 16]


def group_kernel(team_ref, kv_ref, out_ref):
    state = jnp.zeros((8, VDIM), F32)
    decay = jnp.zeros((8, VDIM), F32)
    for member in range(MEMBERS):
        block = team_ref[member, BLOCK:].astype(F32)
        own = joined(block, 16)
        state = state * jnp.exp(own) + joined(block, 0)
        decay = decay + own
    tail = jnp.concatenate([*two_parts(state), *two_parts(decay)], axis=0).astype(BF16)
    kv = kv_ref[...]
    for group in range(GROUPS):
        out_ref[group, 0 : 2 * BLOCK] = kv
        out_ref[group, 2 * BLOCK :] = tail


def attend_kernel(place_ref, weight_ref, team_ref, far_ref, out_ref, key_ref, value_ref):
    group, member = place_ref[0], place_ref[1]
    second_weight = weight_ref[0, 0]
    for other in range(GROUPS):
        span = slice(other * BLOCK, (other + 1) * BLOCK)
        key_ref[span] = far_ref[other, 0:BLOCK]
        value_ref[span, 0:VDIM] = far_ref[other, BLOCK : 2 * BLOCK]
    value_ref[:, VDIM:] = jnp.ones((GROUPS * BLOCK, VDIM), BF16)

    cols = GROUPS * BLOCK
    column = iota((1, cols), 1)
    key_pos = (column // BLOCK * MEMBERS + member) * BLOCK + column % BLOCK
    lane = iota((BLOCK, VDIM), 1)
    logs = jnp.zeros((BLOCK, VDIM), F32)

    def one(index, logs):
        query_pos = (group * MEMBERS + index) * BLOCK + iota((BLOCK, 1), 0)
        causal = key_pos <= query_pos
        found = []
        for which in range(2):
            half = slice(which * HEAD, (which + 1) * HEAD)
            query = team_ref[index, 0:BLOCK, half]
            scores = dot_nt(query, key_ref[:, half])
            scores = jnp.where(causal, scores, NEG_LARGE)
            peak = jnp.max(scores, axis=1, keepdims=True)
            weights = jnp.exp(scores - peak).astype(BF16)
            both = dot(weights, value_ref[...])
            sums = both[:, VDIM:]
            found.append(both[:, :VDIM] / sums)
            logs = jnp.where(lane == 2 * index + which, peak + jnp.log(sums), logs)
        out_ref[index, 0:BLOCK] = found[0].astype(BF16)
        out_ref[index, BLOCK : 2 * BLOCK] = (found[0] - second_weight * found[1]).astype(BF16)
        return logs

    logs = lax.fori_loop(0, MEMBERS, one, logs)

    carried = jnp.zeros((8, VDIM), F32)
    for other in range(GROUPS):
        block = far_ref[other, 2 * BLOCK :].astype(F32)
        carried = jnp.where(
            other < group, carried * jnp.exp(joined(block, 16)) + joined(block, 0), carried
        )
    log_parts = three_parts(logs.T[: 2 * MEMBERS])
    for index in range(MEMBERS):
        pair = slice(2 * index, 2 * index + 2)
        tail = jnp.concatenate(
            [part[pair] for part in log_parts]
            + [jnp.zeros((10, VDIM), F32), *two_parts(carried)],
            axis=0,
        )
        out_ref[index, 2 * BLOCK :] = tail.astype(BF16)
        block = team_ref[index, BLOCK:].astype(F32)
        carried = carried * jnp.exp(joined(block, 16)) + joined(block, 0)


def finish_kernel(
    parts_ref, local_ref, decayed_ref, gate_ref, dgain_ref, lgain_ref, drows_ref, lrows_ref, out_ref
):
    logs, states = [[], []], []
    for member in range(MEMBERS):
        tail = parts_ref[member, 2 * BLOCK :].astype(F32)
        for which in range(2):
            logs[which].append(
                tail[which : which + 1] + tail[which + 2 : which + 3] + tail[which + 4 : which + 5]
            )
        states.append(tail[16:24] + tail[24:32])
    shares = []
    for which in range(2):
        stacked = jnp.concatenate(logs[which], axis=0)
        raised = jnp.exp(stacked - jnp.max(stacked, axis=0, keepdims=True))
        shares.append(raised / jnp.sum(raised, axis=0, keepdims=True))
    factors = jnp.concatenate(
        [shares[0] - shares[1], shares[1], jnp.zeros((BLOCK - 2 * MEMBERS, VDIM), F32)], axis=0
    ).T
    mixed = jnp.zeros((BLOCK, VDIM), F32)
    for member in range(MEMBERS):
        first = parts_ref[member, 0:BLOCK].astype(F32)
        gap = parts_ref[member, BLOCK : 2 * BLOCK].astype(F32)
        mixed = mixed + factors[:, member : member + 1] * first
        mixed = mixed + factors[:, MEMBERS + member : MEMBERS + member + 1] * gap
    mean_sq = jnp.mean(mixed * mixed, axis=1, keepdims=True)
    attn = (0.8 * (mixed * lax.rsqrt(mean_sq + RMS_EPS) * dgain_ref[...])).astype(BF16)

    state = jnp.concatenate(states, axis=0).astype(BF16)
    chain = local_ref[...] + dot(decayed_ref[...], state)
    mean_sq = jnp.mean(chain * chain, axis=1, keepdims=True)
    chain = (chain * lax.rsqrt(mean_sq + RMS_EPS) * lgain_ref[...] * gate_ref[...]).astype(BF16)
    out_ref[...] = (dot(attn, drows_ref[...]) + dot(chain, lrows_ref[...])).astype(BF16)


def call(kernel, outs, scratch=(), scalars=0, inputs=0):
    vmem = pl.BlockSpec(memory_space=pltpu.VMEM)
    smem = pl.BlockSpec(memory_space=pltpu.SMEM)
    return pl.pallas_call(
        kernel,
        in_specs=[smem] * scalars + [vmem] * inputs,
        out_specs=jax.tree.map(lambda _: vmem, outs),
        out_shape=outs,
        scratch_shapes=scratch,
        compiler_params=pltpu.CompilerParams(vmem_limit_bytes=48 * 1024 * 1024),
    )


def exchanged(blocks, axis):
    return lax.all_to_all(blocks, axis, split_axis=0, concat_axis=0, tiled=True)


def per_device(
    tokens, input_norm_gain, differential_query, differential_key, differential_value,
    query_norm_gain, key_norm_gain, second_map_weight, differential_norm_gain, linear_query,
    linear_key, linear_value, linear_output_gate, forget_down_factor, forget_up_factor,
    forget_bias, extra_shrinkage_exponent, linear_norm_gain, differential_output_rows,
    linear_output_rows,
):
    shape = jax.ShapeDtypeStruct
    copies = lax.axis_size("tp")
    rows = exchanged(jnp.broadcast_to(tokens, (copies, *tokens.shape)), "tp")
    place = jnp.stack([lax.axis_index("far"), lax.axis_index(TEAM)]).astype(jnp.int32)

    team, kv, local, decayed, gate = call(
        project_kernel,
        (
            shape((MEMBERS, BLOCK + 32, VDIM), BF16),
            shape((2 * BLOCK, VDIM), BF16),
            shape((BLOCK, VDIM), F32),
            shape((BLOCK, HEAD), BF16),
            shape((BLOCK, VDIM), F32),
        ),
        scratch=[pltpu.VMEM((BLOCK, BLOCK), F32)],
        inputs=15,
    )(
        rows, input_norm_gain.reshape(1, -1), differential_query, differential_key,
        differential_value, linear_query, linear_key, linear_value, linear_output_gate,
        forget_down_factor, forget_up_factor, forget_bias.reshape(1, -1),
        extra_shrinkage_exponent, query_norm_gain.reshape(1, -1), key_norm_gain.reshape(1, -1),
    )
    team = exchanged(team, TEAM)
    far = call(group_kernel, shape((GROUPS, 2 * BLOCK + 32, VDIM), BF16), inputs=2)(team, kv)
    far = exchanged(far, "far")
    parts = call(
        attend_kernel,
        shape((MEMBERS, 2 * BLOCK + 32, VDIM), BF16),
        scratch=[
            pltpu.VMEM((GROUPS * BLOCK, VDIM), BF16),
            pltpu.VMEM((GROUPS * BLOCK, 2 * VDIM), BF16),
        ],
        scalars=1,
        inputs=3,
    )(place, second_map_weight.reshape(1, 1), team, far)
    parts = exchanged(parts, TEAM)
    mixed = call(finish_kernel, shape((BLOCK, differential_output_rows.shape[1]), BF16), inputs=8)(
        parts, local, decayed, gate, differential_norm_gain.reshape(1, -1),
        linear_norm_gain.reshape(1, -1), differential_output_rows, linear_output_rows,
    )
    arrived = exchanged(mixed.reshape(copies, BLOCK // copies, -1), "tp")
    return arrived.astype(F32).sum(axis=0).astype(BF16)


def solution(mesh):
    torus = Mesh(
        mesh.devices.reshape(GROUPS, 2, 4, mesh.shape["tp"]), ("far", "pair", "y", "tp")
    )
    cols, lines = P(None, "tp"), P("tp", None)
    placed = (
        P(SP_TP, None), P(), cols, cols, cols, P(), P(), P("tp"), P(), cols, cols, cols, cols,
        P(), cols, P("tp"), P(SP, "tp"), P(), lines, lines,
    )
    return jax.shard_map(
        per_device, mesh=torus, in_specs=placed, out_specs=P(SP_TP, None), check_vma=False
    )
```

time: 218 us -> 119 us (0.55); the launches traced: 215 us -> 119 us
  waiting for transfers between devices: 93.1 us -> 36.2 us
  blocking collectives: 62.6 us -> 38.5 us
  between operations: 14.5 us -> 0.76 us
  starting transfers between devices: 10.2 us -> 22.7 us
  Pallas kernels: 0 us -> 11 us
  local copies, waits for them, and re-layouts: 18 us -> 8.74 us
  matrix products: 8.6 us -> 0 us
  other arithmetic: 5.59 us -> 0.78 us
  loops' own time: 2.63 us -> 0 us
    all_gather x1 -> x0, waiting for transfers between devices: 91.8 us -> none  [side_by_side(): whole, at, outs = (lax.all_gather(both, axis, axis=dim, tiled=True), 0, [])]
    all_gather x2 -> x0, blocking collectives: 39 us -> none  [all_in_one(): both, at, found = (lax.all_gather(jnp.concatenate(lines), axis), 0, {})]
    all_to_all x1 -> x2, waiting for transfers between devices: 1.25 us -> 36.2 us  [exchanged(): return lax.all_to_all(blocks, axis, split_axis=0, concat_axis=0, tiled=True)]
    all_to_all x1 -> x3, blocking collectives: 23.5 us -> 38.5 us  [exchanged(): return lax.all_to_all(blocks, axis, split_axis=0, concat_axis=0, tiled=True)]
    all_to_all x1 -> x2, starting transfers between devices: 10.2 us -> 22.7 us  [exchanged(): return lax.all_to_all(blocks, axis, split_axis=0, concat_axis=0, tiled=True)]
    pallas_call x0 -> x4, Pallas kernels: none -> 11 us  [the longest x1 6.84 us: per_device(): call(attend_kernel, shape((MEMBERS, 2 * BLOCK + 32, VDIM), BF16), scratch...]
    dot_general x13 -> x0, matrix products: 8.6 us -> none  [the longest x1 3.58 us: per_device(): jnp.dot(gathered_copies(normed, 'tp', 0), packed, preferred_element_type=...]
    concatenate x1 -> x0, local copies, waits for them, and re-layouts: 6.22 us -> none  [per_device(): packed = jnp.concatenate(parts_list, axis=1)]
  transfers between devices with their start and end apart: 2 -> 2, of which waited for: 2 -> 2; matrix products, arithmetic and copies ran while one was open for 5% -> 1% of each run, Pallas kernels for 0% -> 0%
where the time goes in v1:
time: 119 us
  blocking collectives  38.5 us (32%)
  waiting for transfers between devices  36.2 us (30%)
  starting transfers between devices  22.7 us (19%)
  Pallas kernels  11 us (9%)
  local copies, waits for them, and re-layouts  8.74 us (7%)
    all_to_all x3, blocking collectives, exchanged(): return lax.all_to_all(blocks, axis, split_axis=0, concat_axis=0, tiled=True)  38.5 us
    all_to_all x2, waiting for transfers between devices, exchanged(): return lax.all_to_all(blocks, axis, split_axis=0, concat_axis=0, tiled=True)  36.2 us
    all_to_all x2, starting transfers between devices, exchanged(): return lax.all_to_all(blocks, axis, split_axis=0, concat_axis=0, tiled=True)  22.7 us
    unnamed x40, local copies, waits for them, and re-layouts  7.06 us
    pallas_call x1, Pallas kernels, per_device(): call(attend_kernel, shape((MEMBERS, 2 * BLOCK + 32, VDIM), BF16), scratch...  6.84 us
  transfers between devices with their start and end apart: 2, of which 2 were waited for; matrix products, arithmetic and copies ran while one was open for 1% of the time, Pallas kernels for 0%

profile of v1, /device:TPU:1, one launch (start us, length us, event | category | flops | bytes accessed | tf_op | source)
XLA Modules:
  0.0 118.7 jit_solution(15126612459488681977)
XLA Ops:
  0.0 1.7 %broadcast_in_dim.3 = bf16[8,16,2048]{2,1,0:T(8,128)(2,1)} broadcast(bf16[16,2048]{1,0:T(8,128)(2,1)} %param.20), dimensions={1,2} | broadcast | bytes 589824 | tf_op jit(solution)/shard_map/broadcast_in_dim | solution.py:259
  1.7 0.0 copy-start.14
  1.7 10.4 %all-to-all-start = ((bf16[8,16,2048]{2,1,0:T(8,128)(2,1)}), bf16[8,16,2048]{2,1,0:T(8,128)(2,1)S(1)}, u32[]{:S(2)}, u32[]{:S(2)}) async-start(bf16[8,16,2048]{2,1,0:T(8,128)(2,1)} %broadcast_in_dim.3), calls=%async_computation | async-start | bytes 1048576 | tf_op jit(solution)/shard_map/all_to_all | solution.py:247
  12.0 0.0 copy-done.14
  12.1 0.0 copy-start.15
  12.1 0.3 copy.21.lq_ref
  12.3 0.7 copy-done.15
  13.0 0.0 copy-start.16
  13.0 0.0 copy-start.3
  13.0 0.3 copy.22.lk_ref
  13.3 0.6 copy-done.16
  13.9 0.0 copy-start.17
  13.9 0.0 copy-start.2
  13.9 0.3 copy.23.down_ref
  14.2 0.4 copy-done.17
  14.6 0.0 copy-start.7
  14.6 0.0 copy-start.8
  14.6 0.1 copy.24.shrink_ref
  14.7 6.7 %all-to-all-done.rows_ref = bf16[8,16,2048]{2,1,0:T(8,128)(2,1)S(1)} async-done(((bf16[8,16,2048]{2,1,0:T(8,128)(2,1)}), bf16[8,16,2048]{2,1,0:T(8,128)(2,1)S(1)}, u32[]{:S(2)}, u32[]{:S(2)}) %all-to-all-start) | async-done | bytes 524320 | tf_op jit(solution)/shard_map/all_to_all | solution.py:247
  21.4 0.0 copy-start.9
  21.4 0.0 copy-start.10
  21.4 0.0 copy-start.11
  21.4 0.0 copy-done.3
  21.4 0.0 copy-done.2
  21.4 0.0 copy-done.7
  21.5 0.0 copy-done.8
  21.5 0.6 copy-done.9
  22.1 0.0 copy-done.10
  22.1 0.0 copy-done.11
  22.1 0.0 copy-start.4
  22.1 1.0 copy-done.4
  23.2 0.0 copy-start.5
  23.2 1.0 copy-done.5
  24.2 0.0 copy-start.6
  24.2 1.0 copy-done.6
  25.2 2.2 %shard_map.190 = (bf16[8,160,128]{2,1,0:T(8,128)(2,1)S(1)}, bf16[256,128]{1,0:T(8,128)(2,1)S(1)}, f32[128,128]{1,0:T(8,128)S(1)}, bf16[128,64]{1,0:T(8,128)(2,1)S(1)}, f32[128,128]{1,0:T(8,128)S(1)}) custom-call(bf16[8,16,2048]{2,1,0:T(8,128)(2,1)S(1)} %all-to-all-done.rows_ref, f32[1,2048]{1,0:T(1,128)S(1)} %bitcast.12, bf16[2048,128]{1,0:T(8,128)(2,1)S(1)} %copy-done.2, ...), custom_call_target="tpu_custom_call" | custom-call | tf_op jit(solution)/shard_map/pallas_call | solution.py:262
  27.5 9.1 %all_to_all.25.team_ref = bf16[8,160,128]{2,1,0:T(8,128)(2,1)S(1)} all-to-all(bf16[8,160,128]{2,1,0:T(8,128)(2,1)S(1)} %get-tuple-element.10), channel_id=1, replica_groups=mesh['far'=8,'pair'=2,'y'=4,'tp'=8] {'pair','y'}, dimensions={0} | all-to-all | bytes 655360 | tf_op jit(solution)/shard_map/all_to_all | solution.py:247
  36.6 0.9 shard_map.191
  37.5 12.3 %all-to-all-start.2 = ((bf16[8,288,128]{2,1,0:T(8,128)(2,1)}), bf16[8,288,128]{2,1,0:T(8,128)(2,1)S(1)}, u32[]{:S(2)}, u32[]{:S(2)}) async-start(bf16[8,288,128]{2,1,0:T(8,128)(2,1)} %shard_map.191), calls=%async_computation.2 | async-start | bytes 1179648 | tf_op jit(solution)/shard_map/all_to_all | solution.py:247
  50.5 0.1 pad_add_fusion.place_ref
  50.6 29.5 %all-to-all-done.2.far_ref = bf16[8,288,128]{2,1,0:T(8,128)(2,1)S(1)} async-done(((bf16[8,288,128]{2,1,0:T(8,128)(2,1)}), bf16[8,288,128]{2,1,0:T(8,128)(2,1)S(1)}, u32[]{:S(2)}, u32[]{:S(2)}) %all-to-all-start.2) | async-done | bytes 589856 | tf_op jit(solution)/shard_map/all_to_all | solution.py:247
  80.1 6.8 %shard_map.192 = bf16[8,288,128]{2,1,0:T(8,128)(2,1)S(1)} custom-call(s32[2]{0:T(128)S(1)} %pad_add_fusion.place_ref, f32[1,1]{1,0:T(1,128)} %bitcast.10.weight_ref, bf16[8,160,128]{2,1,0:T(8,128)(2,1)S(1)} %all_to_all.25.team_ref, bf16[8,288,128]{2,1,0:T(8,128)(2,1)S(1)} %all-to-all-done.2.far_ref), custom_call_target="tpu_custom_call" | custom-call | tf_op jit(solution)/shard_map/pallas_call | solution.py:282
  86.9 0.0 copy-start
  86.9 0.0 copy-start.1
  86.9 11.0 %all_to_all.26.parts_ref = bf16[8,288,128]{2,1,0:T(8,128)(2,1)S(1)} all-to-all(bf16[8,288,128]{2,1,0:T(8,128)(2,1)S(1)} %shard_map.192), channel_id=1, replica_groups=mesh['far'=8,'pair'=2,'y'=4,'tp'=8] {'pair','y'}, dimensions={0} | all-to-all | bytes 1179648 | tf_op jit(solution)/shard_map/all_to_all | solution.py:247
  98.0 0.0 copy-start.12
  98.0 0.0 copy-start.13
  98.0 0.0 copy-done
  98.0 0.0 copy-done.1
  98.0 0.6 copy-done.12
  98.6 0.0 copy-done.13
  98.6 1.0 shard_map.193
  99.6 18.4 %all_to_all.27 = bf16[8,16,2048]{2,1,0:T(8,128)(2,1)S(1)} all-to-all(bf16[8,16,2048]{2,1,0:T(8,128)(2,1)S(1)} %bitcast.11), channel_id=1, replica_groups=mesh['far'=8,'pair'=2,'y'=4,'tp'=8] {'tp'}, dimensions={0} | all-to-all | bytes 1048576 | tf_op jit(solution)/shard_map/all_to_all | solution.py:247
  118.0 0.7 reduce_sum.12
Async XLA Ops:
  1.7 10.4 %copy-start.14 = (bf16[2048,64]{0,1:T(8,128)(2,1)S(1)}, bf16[2048,64]{0,1:T(8,128)(2,1)}, u32[]{:S(2)}) copy-start(bf16[2048,64]{0,1:T(8,128)(2,1)} %param.29) | copy-start | bytes 786436
  1.7 19.7 %all-to-all-start = ((bf16[8,16,2048]{2,1,0:T(8,128)(2,1)}), bf16[8,16,2048]{2,1,0:T(8,128)(2,1)S(1)}, u32[]{:S(2)}, u32[]{:S(2)}) async-start(bf16[8,16,2048]{2,1,0:T(8,128)(2,1)} %broadcast_in_dim.3), calls=%async_computation | async-start | bytes 1048576 | tf_op jit(solution)/shard_map/all_to_all | solution.py:247
  12.1 1.0 copy-start.15
  13.0 0.9 copy-start.16
  13.0 8.4 %copy-start.3 = (bf16[2048,128]{1,0:T(8,128)(2,1)S(1)}, bf16[2048,128]{1,0:T(8,128)(2,1)}, u32[]{:S(2)}) copy-start(bf16[2048,128]{1,0:T(8,128)(2,1)} %dk_ref.1) | copy-start | bytes 1572868
  13.9 0.7 copy-start.17
  13.9 7.5 %copy-start.2 = (bf16[2048,128]{1,0:T(8,128)(2,1)S(1)}, bf16[2048,128]{1,0:T(8,128)(2,1)}, u32[]{:S(2)}) copy-start(bf16[2048,128]{1,0:T(8,128)(2,1)} %dq_ref.1) | copy-start | bytes 1572868
  14.6 6.9 %copy-start.7 = (f32[2048]{0:T(1024)S(1)}, f32[2048]{0:T(1024)}, u32[]{:S(2)}) copy-start(f32[2048]{0:T(1024)} %param.21) | copy-start | bytes 24580
  14.6 6.9 %copy-start.8 = (bf16[32,64]{1,0:T(8,128)(2,1)S(1)}, bf16[32,64]{1,0:T(8,128)(2,1)}, u32[]{:S(2)}) copy-start(bf16[32,64]{1,0:T(8,128)(2,1)} %up_ref.1) | copy-start | bytes 12292
  21.4 0.7 copy-start.9
  21.4 0.7 copy-start.10
  21.4 0.7 copy-start.11
  22.1 1.0 copy-start.4
  23.2 1.0 copy-start.5
  24.2 1.0 copy-start.6
  37.5 42.5 %all-to-all-start.2 = ((bf16[8,288,128]{2,1,0:T(8,128)(2,1)}), bf16[8,288,128]{2,1,0:T(8,128)(2,1)S(1)}, u32[]{:S(2)}, u32[]{:S(2)}) async-start(bf16[8,288,128]{2,1,0:T(8,128)(2,1)} %shard_map.191), calls=%async_computation.2 | async-start | bytes 1179648 | tf_op jit(solution)/shard_map/all_to_all | solution.py:247
  86.9 11.0 %copy-start = (bf16[128,2048]{1,0:T(8,128)(2,1)S(1)}, bf16[128,2048]{1,0:T(8,128)(2,1)}, u32[]{:S(2)}) copy-start(bf16[128,2048]{1,0:T(8,128)(2,1)} %drows_ref.1) | copy-start | bytes 1572868
  86.9 11.0 %copy-start.1 = (bf16[128,2048]{1,0:T(8,128)(2,1)S(1)}, bf16[128,2048]{1,0:T(8,128)(2,1)}, u32[]{:S(2)}) copy-start(bf16[128,2048]{1,0:T(8,128)(2,1)} %lrows_ref.1) | copy-start | bytes 1572868
  98.0 0.7 copy-start.12
  98.0 0.7 copy-start.13

commit v2 on v1

v2 whole, which is shorter than its diff:
```python
import jax
import jax.numpy as jnp
from jax import lax
from jax.experimental import pallas as pl
from jax.experimental.pallas import tpu as pltpu
from jax.sharding import Mesh
from jax.sharding import PartitionSpec as P

F32 = jnp.float32
BF16 = jnp.bfloat16
HEAD = 64
VDIM = 128
BLOCK = 128
SUB = 16
GROUPS = 8
MEMBERS = 8
SP = ("far", "pair", "y")
TEAM = ("pair", "y")
TP = ("x", "core")
SP_TP = ("far", "pair", "y", "x", "core")
RMS_EPS = 1e-06
NEG_LARGE = -1e30
NT = (((1,), (1,)), ((), ()))


def two_parts(x):
    high = x.astype(BF16).astype(F32)
    return high, (x - high).astype(BF16).astype(F32)


def three_parts(x):
    high, rest = x.astype(BF16).astype(F32), None
    middle = (x - high).astype(BF16).astype(F32)
    rest = ((x - high) - middle).astype(BF16).astype(F32)
    return high, middle, rest


def dot(a, b):
    return jnp.dot(a, b, preferred_element_type=F32)


def dot_nt(a, b):
    return lax.dot_general(a, b, NT, preferred_element_type=F32)


def iota(shape, dim):
    return lax.broadcasted_iota(jnp.int32, shape, dim)


def two_map_norm(values, gain):
    first = iota(values.shape, 1) < HEAD
    squares = values * values
    low = jnp.sum(jnp.where(first, squares, 0.0), axis=1, keepdims=True)
    high = jnp.sum(jnp.where(first, 0.0, squares), axis=1, keepdims=True)
    mean_sq = jnp.where(first, low, high) * (1.0 / HEAD)
    return values * lax.rsqrt(mean_sq + RMS_EPS) * gain


def prepare_kernel(
    bias_ref, shrink_ref, qgain_ref, kgain_ref, dgain_ref, lgain_ref, gain_ref, up_ref,
    small_ref, shrunk_ref, ready_gain_ref, ready_up_ref,
):
    small_ref[0:1] = jnp.concatenate([qgain_ref[...]] * 2, axis=1)
    small_ref[1:2] = jnp.concatenate([kgain_ref[...]] * 2, axis=1)
    small_ref[2:3] = jnp.concatenate([bias_ref[...]] * 2, axis=1)
    small_ref[3:4] = dgain_ref[...]
    small_ref[4:5] = lgain_ref[...]
    small_ref[5:] = jnp.zeros((3, VDIM), F32)
    shrunk_ref[...] = jnp.broadcast_to(shrink_ref[...], shrunk_ref.shape).T
    ready_gain_ref[...] = gain_ref[...]
    ready_up_ref[...] = up_ref[...]


def project_kernel(
    rows_ref, gain_ref, dq_ref, lv_ref, lk_ref, down_ref, small_ref, shrunk_ref, up_ref,
    team_ref, normed_ref, lk_out_ref, lv_out_ref, total_ref,
):
    rows = jnp.concatenate(
        [rows_ref[core, chip] for chip in range(rows_ref.shape[1]) for core in range(2)], axis=0
    ).astype(F32)
    mean_sq = jnp.mean(rows * rows, axis=1, keepdims=True)
    normed = (rows * lax.rsqrt(mean_sq + RMS_EPS) * gain_ref[...]).astype(BF16)
    normed_ref[...] = normed

    lk = dot_nt(normed, lk_ref[...]).astype(BF16)
    low = dot_nt(normed, down_ref[...]).astype(BF16)
    lv = dot(normed, lv_ref[...]).astype(BF16)
    lk_out_ref[...] = lk
    lv_out_ref[...] = lv

    query = two_map_norm(dot(normed, dq_ref[...]).astype(BF16).astype(F32), small_ref[0:1])
    query = query.astype(BF16) * jnp.asarray(HEAD**-0.5, BF16)

    pre = dot(low, up_ref[...]) + small_ref[2:3, 0:HEAD]
    log_sig = jnp.minimum(pre, 0.0) - jnp.log1p(jnp.exp(-jnp.abs(pre)))
    log_a = log_sig * (1.0 / 16.0) + shrunk_ref[:, 0:HEAD]
    lower = (iota((BLOCK, BLOCK), 0) >= iota((BLOCK, BLOCK), 1)).astype(BF16)
    total = sum(dot(lower, piece.astype(BF16)) for piece in three_parts(log_a))

    total_ref[...] = total
    k_end = lk.astype(F32) * jnp.exp(total[BLOCK - 1 :] - total)
    flipped = jnp.concatenate([total, k_end], axis=1).T
    decay = jnp.broadcast_to(flipped[:HEAD, BLOCK - 1 :], (HEAD, VDIM))
    state = dot(flipped[HEAD:].astype(BF16), lv)
    state_parts = two_parts(state)
    decay_parts = two_parts(decay)
    for member in range(MEMBERS):
        own = slice(member * 8, member * 8 + 8)
        team_ref[member, 0:BLOCK] = query
        team_ref[member, BLOCK:] = jnp.concatenate(
            [piece[own] for piece in (*state_parts, *decay_parts)], axis=0
        ).astype(BF16)


def key_value_kernel(normed_ref, dk_ref, dv_ref, small_ref, kv_ref):
    normed = normed_ref[...]
    key = two_map_norm(dot(normed, dk_ref[...]).astype(BF16).astype(F32), small_ref[1:2])
    kv_ref[0:BLOCK] = key.astype(BF16)
    kv_ref[BLOCK:] = dot(normed, dv_ref[...]).astype(BF16)


def local_kernel(
    normed_ref, lg_ref, lq_ref, lk_ref, lv_ref, total_ref, local_ref, decayed_ref, gate_ref,
    scores_ref,
):
    gate = dot(normed_ref[...], lg_ref[...]).astype(BF16).astype(F32)
    gate_ref[...] = gate * jax.nn.sigmoid(gate)
    lq = dot_nt(normed_ref[...], lq_ref[...]).astype(BF16).astype(F32) * HEAD**-0.5
    lk = lk_ref[...].astype(F32)
    lv = lv_ref[...]
    total = total_ref[...]
    scores_ref[...] = jnp.zeros_like(scores_ref)
    for step in range(1, BLOCK // SUB):
        at = step * SUB
        border = total[at - 1 : at]
        q_part = lq[at : at + SUB] * jnp.exp(total[at : at + SUB] - border)
        k_part = lk[:at] * jnp.exp(border - total[:at])
        scores_ref[at : at + SUB, 0:at] = dot_nt(q_part.astype(BF16), k_part.astype(BF16))
    scores = scores_ref[...]
    row = iota((BLOCK, BLOCK), 0)
    distance = row - iota((BLOCK, BLOCK), 1)
    for shift in range(SUB):
        k_part = lk if shift == 0 else pltpu.roll(lk, shift, 0)
        if shift == 0:
            terms = lq * k_part
        else:
            terms = lq * k_part * jnp.exp(jnp.minimum(total - pltpu.roll(total, shift, 0), 0.0))
        column = jnp.sum(terms, axis=1, keepdims=True)
        here = (distance == shift) & (row % SUB >= shift)
        scores = jnp.where(here, column, scores)
    local_ref[...] = dot(scores.astype(BF16), lv)
    decayed_ref[...] = (lq * jnp.exp(total)).astype(BF16)


def joined(block, at):
    return block[at : at + 8] + block[at + 8 : at + 16]


def group_kernel(team_ref, kv_ref, out_ref):
    state = jnp.zeros((8, VDIM), F32)
    decay = jnp.zeros((8, VDIM), F32)
    for member in range(MEMBERS):
        block = team_ref[member, BLOCK:].astype(F32)
        own = joined(block, 16)
        state = state * jnp.exp(own) + joined(block, 0)
        decay = decay + own
    tail = jnp.concatenate([*two_parts(state), *two_parts(decay)], axis=0).astype(BF16)
    out_ref[0 : 2 * BLOCK] = kv_ref[...]
    out_ref[2 * BLOCK :] = tail


def attend_kernel(
    place_ref, weight_ref, team_ref, far_ref, out_ref, query_ref, key_ref, value_ref, logs_ref
):
    group, member = place_ref[0], place_ref[1]
    second_weight = weight_ref[0, 0]
    for other in range(GROUPS):
        span = slice(other * BLOCK, (other + 1) * BLOCK)
        query_ref[span] = team_ref[other, 0:BLOCK]
        key_ref[span] = far_ref[other, 0:BLOCK]
        value_ref[span, 0:VDIM] = far_ref[other, BLOCK : 2 * BLOCK]
    value_ref[:, VDIM:] = jnp.ones((GROUPS * BLOCK, VDIM), BF16)

    column = iota((1, 2 * BLOCK), 1)
    key_pos = (column // BLOCK * MEMBERS + member) * BLOCK + column % BLOCK
    lane = iota((BLOCK, VDIM), 1)
    logs_ref[...] = jnp.zeros_like(logs_ref)

    def attend(blocks):
        cols, open_cols = blocks * BLOCK, (blocks - 2) * BLOCK
        last_pos = key_pos + (blocks - 2) * MEMBERS * BLOCK
        batch = {2: 8, 4: 4}.get(blocks, 2)
        rows = batch * BLOCK

        def one(step, _):
            start = pl.multiple_of(step * rows, rows)
            causal = last_pos <= group * MEMBERS * BLOCK + start + iota((rows, 1), 0)
            found, logs = [], []
            for which in range(2):
                half = slice(which * HEAD, (which + 1) * HEAD)
                query = query_ref[pl.ds(start, rows), half]
                scores = dot_nt(query, key_ref[open_cols:cols, half])
                scores = jnp.where(causal, scores, NEG_LARGE)
                if open_cols:
                    scores = jnp.concatenate(
                        [dot_nt(query, key_ref[0:open_cols, half]), scores], axis=1
                    )
                peak = jnp.max(scores, axis=1, keepdims=True)
                weights = jnp.exp(scores - peak).astype(BF16)
                both = dot(weights, value_ref[0:cols])
                sums = both[:, VDIM:]
                found.append(both[:, :VDIM] / sums)
                logs.append(peak + jnp.log(sums))
            gap = found[0] - second_weight * found[1]
            total = logs_ref[...]
            for near in range(batch):
                index = step * batch + near
                part = slice(near * BLOCK, (near + 1) * BLOCK)
                out_ref[index, 0:BLOCK] = found[0][part].astype(BF16)
                out_ref[index, BLOCK : 2 * BLOCK] = gap[part].astype(BF16)
                for which in range(2):
                    total = jnp.where(lane == 2 * index + which, logs[which][part], total)
            logs_ref[...] = total
            return _

        if batch == MEMBERS:
            one(0, 0)
        else:
            lax.fori_loop(0, MEMBERS // batch, one, 0)

    for blocks in range(2, GROUPS + 1, 2):
        pl.when(group // 2 == blocks // 2 - 1)(lambda blocks=blocks: attend(blocks))
    logs = logs_ref[...]

    carried = jnp.zeros((8, VDIM), F32)
    for other in range(GROUPS):
        block = far_ref[other, 2 * BLOCK :].astype(F32)
        carried = jnp.where(
            other < group, carried * jnp.exp(joined(block, 16)) + joined(block, 0), carried
        )
    log_parts = three_parts(logs.T[: 2 * MEMBERS])
    for index in range(MEMBERS):
        pair = slice(2 * index, 2 * index + 2)
        tail = jnp.concatenate(
            [part[pair] for part in log_parts]
            + [jnp.zeros((10, VDIM), F32), *two_parts(carried)],
            axis=0,
        )
        out_ref[index, 2 * BLOCK :] = tail.astype(BF16)
        block = team_ref[index, BLOCK:].astype(F32)
        carried = carried * jnp.exp(joined(block, 16)) + joined(block, 0)


def finish_kernel(
    parts_ref, local_ref, decayed_ref, gate_ref, small_ref, drows_ref, lrows_ref, out_ref
):
    logs, states = [[], []], []
    for member in range(MEMBERS):
        tail = parts_ref[member, 2 * BLOCK :].astype(F32)
        for which in range(2):
            logs[which].append(
                tail[which : which + 1] + tail[which + 2 : which + 3] + tail[which + 4 : which + 5]
            )
        states.append(tail[16:24] + tail[24:32])
    shares = []
    for which in range(2):
        stacked = jnp.concatenate(logs[which], axis=0)
        raised = jnp.exp(stacked - jnp.max(stacked, axis=0, keepdims=True))
        shares.append(raised / jnp.sum(raised, axis=0, keepdims=True))
    factors = jnp.concatenate(
        [shares[0] - shares[1], shares[1], jnp.zeros((BLOCK - 2 * MEMBERS, VDIM), F32)], axis=0
    ).T
    mixed = jnp.zeros((BLOCK, VDIM), F32)
    for member in range(MEMBERS):
        first = parts_ref[member, 0:BLOCK].astype(F32)
        gap = parts_ref[member, BLOCK : 2 * BLOCK].astype(F32)
        mixed = mixed + factors[:, member : member + 1] * first
        mixed = mixed + factors[:, MEMBERS + member : MEMBERS + member + 1] * gap
    mean_sq = jnp.mean(mixed * mixed, axis=1, keepdims=True)
    attn = (0.8 * (mixed * lax.rsqrt(mean_sq + RMS_EPS) * small_ref[3:4])).astype(BF16)

    state = jnp.concatenate(states, axis=0).astype(BF16)
    chain = local_ref[...] + dot(decayed_ref[...], state)
    mean_sq = jnp.mean(chain * chain, axis=1, keepdims=True)
    chain = (chain * lax.rsqrt(mean_sq + RMS_EPS) * small_ref[4:5] * gate_ref[...]).astype(BF16)
    out_ref[...] = (dot(attn, drows_ref[...]) + dot(chain, lrows_ref[...])).astype(BF16)


def call(kernel, outs, scratch=(), scalars=0, inputs=0):
    vmem = pl.BlockSpec(memory_space=pltpu.VMEM)
    smem = pl.BlockSpec(memory_space=pltpu.SMEM)
    return pl.pallas_call(
        kernel,
        in_specs=[smem] * scalars + [vmem] * inputs,
        out_specs=jax.tree.map(lambda _: vmem, outs),
        out_shape=outs,
        scratch_shapes=scratch,
        compiler_params=pltpu.CompilerParams(vmem_limit_bytes=48 * 2**20),
    )


def exchanged(blocks, axis):
    return lax.all_to_all(blocks, axis, split_axis=0, concat_axis=0, tiled=True)


def per_device(
    tokens, input_norm_gain, differential_query, differential_key, differential_value,
    query_norm_gain, key_norm_gain, second_map_weight, differential_norm_gain, linear_query,
    linear_key, linear_value, linear_output_gate, forget_down_factor, forget_up_factor,
    forget_bias, extra_shrinkage_exponent, linear_norm_gain, differential_output_rows,
    linear_output_rows,
):
    shape = jax.ShapeDtypeStruct
    copies = lax.axis_size(TP)
    rows = exchanged(jnp.broadcast_to(tokens, (copies // 2, *tokens.shape)), "x")
    rows = lax.all_gather(rows, "core")
    place = jnp.stack([lax.axis_index("far"), lax.axis_index(TEAM)]).astype(jnp.int32)

    features = tokens.shape[1]
    small, shrunk, gain, up = call(
        prepare_kernel,
        (
            shape((8, VDIM), F32),
            shape((BLOCK, VDIM), F32),
            shape((1, features), F32),
            shape(forget_up_factor.shape, BF16),
        ),
        inputs=8,
    )(
        forget_bias.reshape(1, -1), extra_shrinkage_exponent.reshape(1, -1),
        query_norm_gain.reshape(1, -1), key_norm_gain.reshape(1, -1),
        differential_norm_gain.reshape(1, -1), linear_norm_gain.reshape(1, -1),
        input_norm_gain.reshape(1, -1), forget_up_factor,
    )
    team, normed, lk, lv, total = call(
        project_kernel,
        (
            shape((MEMBERS, BLOCK + 32, VDIM), BF16),
            shape((BLOCK, features), BF16),
            shape((BLOCK, HEAD), BF16),
            shape((BLOCK, VDIM), BF16),
            shape((BLOCK, HEAD), F32),
        ),
        inputs=9,
    )(
        rows, gain, differential_query, linear_value, linear_key.T, forget_down_factor.T, small,
        shrunk, up,
    )
    kv = call(key_value_kernel, shape((2 * BLOCK, VDIM), BF16), inputs=4)(
        normed, differential_key, differential_value, small
    )
    local, decayed, gate = call(
        local_kernel,
        (
            shape((BLOCK, VDIM), F32),
            shape((BLOCK, HEAD), BF16),
            shape((BLOCK, VDIM), F32),
        ),
        scratch=[pltpu.VMEM((BLOCK, BLOCK), F32)],
        inputs=6,
    )(normed, linear_output_gate, linear_query.T, lk, lv, total)
    team = exchanged(team, TEAM)
    far = call(group_kernel, shape((2 * BLOCK + 32, VDIM), BF16), inputs=2)(team, kv)
    far = lax.all_gather(far, "far")
    parts = call(
        attend_kernel,
        shape((MEMBERS, 2 * BLOCK + 32, VDIM), BF16),
        scratch=[
            pltpu.VMEM((MEMBERS * BLOCK, VDIM), BF16),
            pltpu.VMEM((GROUPS * BLOCK, VDIM), BF16),
            pltpu.VMEM((GROUPS * BLOCK, 2 * VDIM), BF16),
            pltpu.VMEM((BLOCK, VDIM), F32),
        ],
        scalars=1,
        inputs=3,
    )(place, second_map_weight.reshape(1, 1), team, far)
    parts = exchanged(parts, TEAM)
    mixed = call(finish_kernel, shape((BLOCK, differential_output_rows.shape[1]), BF16), inputs=7)(
        parts, local, decayed, gate, small, differential_output_rows, linear_output_rows
    )
    arrived = exchanged(mixed.reshape(copies, BLOCK // copies, -1), TP)
    return arrived.astype(F32).sum(axis=0).astype(BF16)


def solution(mesh):
    torus = Mesh(
        mesh.devices.reshape(GROUPS, 2, 4, mesh.shape["tp"] // 2, 2),
        ("far", "pair", "y", "x", "core"),
    )
    cols, lines = P(None, TP), P(TP, None)
    placed = (
        P(SP_TP, None), P(), cols, cols, cols, P(), P(), P(TP), P(), cols, cols, cols, cols,
        P(), cols, P(TP), P(SP, TP), P(), lines, lines,
    )
    return jax.shard_map(
        per_device, mesh=torus, in_specs=placed, out_specs=P(SP_TP, None), check_vma=False
    )
```

time: 119 us -> 99.1 us (0.83)
  waiting for transfers between devices: 36.2 us -> 17 us
  blocking collectives: 38.5 us -> 57.3 us
  starting transfers between devices: 22.7 us -> 13.1 us
  local copies, waits for them, and re-layouts: 8.74 us -> 1.69 us
  Pallas kernels: 11 us -> 7.89 us
    all_gather x0 -> x2, blocking collectives: none -> 37.4 us  [the longest x1 29 us: per_device(): far = lax.all_gather(far, 'far')]
    all_to_all x2 -> x3, waiting for transfers between devices: 36.2 us -> 17 us  [exchanged(): return lax.all_to_all(blocks, axis, split_axis=0, concat_axis=0, tiled=True)]
    all_to_all x3 -> x1, blocking collectives: 38.5 us -> 19.9 us  [exchanged(): return lax.all_to_all(blocks, axis, split_axis=0, concat_axis=0, tiled=True)]
    all_to_all x2 -> x3, starting transfers between devices: 22.7 us -> 13.1 us  [exchanged(): return lax.all_to_all(blocks, axis, split_axis=0, concat_axis=0, tiled=True)]
    unnamed x40 -> x36, local copies, waits for them, and re-layouts: 7.06 us -> 0.09 us
    pallas_call x1, Pallas kernels: 6.84 us -> 3.2 us  [per_device(): call(attend_kernel, shape((MEMBERS, 2 * BLOCK + 32, VDIM), BF16), scratch...]
    pallas_call x2 -> x5, Pallas kernels: 3.14 us -> 3.69 us  [the longest x1 2.17 us: per_device(): call(project_kernel, (shape((MEMBERS, BLOCK + 32, VDIM), BF16), shape((BL...]
  transfers between devices with their start and end apart: 2 -> 3, of which waited for: 2 -> 3; matrix products, arithmetic and copies ran while one was open for 1% -> 0% of each run, Pallas kernels for 0% -> 2%
where the time goes in v2:
time: 99.1 us; the launch traced here: 98.6 us
  blocking collectives  57.3 us (58%)
  waiting for transfers between devices  17 us (17%)
  starting transfers between devices  13.1 us (13%)
  Pallas kernels  7.89 us (8%)
  local copies, waits for them, and re-layouts  1.69 us (2%)
    all_gather x1, blocking collectives, per_device(): far = lax.all_gather(far, 'far')  29 us
    all_to_all x1, blocking collectives, exchanged(): return lax.all_to_all(blocks, axis, split_axis=0, concat_axis=0, tiled=True)  19.9 us
    all_to_all x3, waiting for transfers between devices, exchanged(): return lax.all_to_all(blocks, axis, split_axis=0, concat_axis=0, tiled=True)  17 us
    all_to_all x3, starting transfers between devices, exchanged(): return lax.all_to_all(blocks, axis, split_axis=0, concat_axis=0, tiled=True)  13.1 us
    all_gather x1, blocking collectives, per_device(): rows = lax.all_gather(rows, 'core')  8.33 us
    pallas_call x1, Pallas kernels, per_device(): call(attend_kernel, shape((MEMBERS, 2 * BLOCK + 32, VDIM), BF16), scratch...  3.2 us
    pallas_call x1, Pallas kernels, per_device(): call(project_kernel, (shape((MEMBERS, BLOCK + 32, VDIM), BF16), shape((BL...  2.17 us
  transfers between devices with their start and end apart: 3, of which 3 were waited for; matrix products, arithmetic and copies ran while one was open for 0% of the time, Pallas kernels for 2%

profile of v2, /device:TPU:1, one launch (start us, length us, event | category | flops | bytes accessed | tf_op | source)
XLA Modules:
  0.0 98.6 jit_solution(13026751964314590819)
XLA Ops:
  0.0 0.0 copy-start.11
  0.0 0.0 copy-start.9
  0.0 1.6 %broadcast_in_dim.3 = bf16[4,16,2048]{2,1,0:T(8,128)(2,1)} broadcast(bf16[16,2048]{1,0:T(8,128)(2,1)} %param.20), dimensions={1,2} | broadcast | bytes 327680 | tf_op jit(solution)/shard_map/broadcast_in_dim | solution.py:315
  1.6 0.0 copy-start.10
  1.6 0.0 copy-start.12
  1.6 0.0 copy-start.13
  1.6 0.0 copy-start.14
  1.6 0.0 copy-start.15
  1.6 0.0 copy-start.16
  1.6 0.0 copy-start.17
  1.7 0.0 copy-start.3
  1.7 5.0 %all-to-all-start = ((bf16[4,16,2048]{2,1,0:T(8,128)(2,1)}), bf16[4,16,2048]{2,1,0:T(8,128)(2,1)S(1)}, u32[]{:S(2)}, u32[]{:S(2)}) async-start(bf16[4,16,2048]{2,1,0:T(8,128)(2,1)} %broadcast_in_dim.3), calls=%async_computation | async-start | bytes 524288 | tf_op jit(solution)/shard_map/all_to_all | solution.py:303
  6.6 0.0 copy-start.2
  6.6 0.0 copy-done.11
  6.6 0.0 copy-done.10
  6.7 0.0 copy-done.12
  6.7 0.0 copy-done.13
  6.7 0.0 copy-done.14
  6.7 0.0 copy-done.15
  6.7 0.0 copy-done.16
  6.7 0.0 copy-done.17
  6.7 0.1 shard_map.190
  6.8 0.0 copy-start.8
  6.8 5.3 %all-to-all-done = bf16[4,16,2048]{2,1,0:T(8,128)(2,1)S(1)} async-done(((bf16[4,16,2048]{2,1,0:T(8,128)(2,1)}), bf16[4,16,2048]{2,1,0:T(8,128)(2,1)S(1)}, u32[]{:S(2)}, u32[]{:S(2)}) %all-to-all-start) | async-done | bytes 262176 | tf_op jit(solution)/shard_map/all_to_all | solution.py:303
  12.2 8.3 %all-gather = bf16[8,16,2048]{2,1,0:T(8,128)(2,1)S(1)} all-gather(bf16[4,16,2048]{2,1,0:T(8,128)(2,1)S(1)} %all-to-all-done), channel_id=2, replica_groups=mesh['far'=8,'pair'=2,'y'=4,'x'=4,'core'=2] {'core'}, dimensions={0}, use_global_device_ids=true | all-gather | bytes 786432 | tf_op jit(solution)/shard_map/all_gather | solution.py:316
  20.5 0.0 copy-done.9
  20.5 0.0 copy-done.3
  20.5 0.0 copy-done.2
  20.5 0.0 copy-done.8
  20.5 0.0 copy-start.1
  20.5 2.2 %shard_map.191 = (bf16[8,160,128]{2,1,0:T(8,128)(2,1)}, bf16[128,2048]{1,0:T(8,128)(2,1)S(1)}, bf16[128,64]{1,0:T(8,128)(2,1)S(1)}, bf16[128,128]{1,0:T(8,128)(2,1)S(1)}, f32[128,64]{1,0:T(8,128)S(1)}) custom-call(bf16[2,4,16,2048]{3,2,1,0:T(8,128)(2,1)S(1)} %bitcast.18, f32[1,2048]{1,0:T(1,128)S(1)} %get-tuple-element.17.gain_ref, ...), custom_call_target="tpu_custom_call" | custom-call | tf_op jit(solution)/shard_map/pallas_call | solution.py:335
  22.7 0.0 copy-start
  22.7 3.6 %all-to-all-start.1 = ((bf16[8,160,128]{2,1,0:T(8,128)(2,1)}), bf16[8,160,128]{2,1,0:T(8,128)(2,1)S(1)}, u32[]{:S(2)}, u32[]{:S(2)}) async-start(bf16[8,160,128]{2,1,0:T(8,128)(2,1)} %get-tuple-element.21), calls=%async_computation.1 | async-start | bytes 655360 | tf_op jit(solution)/shard_map/all_to_all | solution.py:303
  26.9 0.1 pad_add_fusion.place_ref
  27.0 0.0 copy-done.1
  27.0 0.0 copy-done
  27.0 0.4 shard_map.192.kv_ref
  27.4 5.3 %all-to-all-done.1.team_ref = bf16[8,160,128]{2,1,0:T(8,128)(2,1)S(1)} async-done(((bf16[8,160,128]{2,1,0:T(8,128)(2,1)}), bf16[8,160,128]{2,1,0:T(8,128)(2,1)S(1)}, u32[]{:S(2)}, u32[]{:S(2)}) %all-to-all-start.1) | async-done | bytes 327712 | tf_op jit(solution)/shard_map/all_to_all | solution.py:303
  32.8 29.0 %all-gather.1 = bf16[2304,128]{1,0:T(8,128)(2,1)S(1)} all-gather(bf16[288,128]{1,0:T(8,128)(2,1)S(1)} %shard_map.193), channel_id=3, replica_groups=mesh['far'=8,'pair'=2,'y'=4,'x'=4,'core'=2] {'far'}, dimensions={0}, use_global_device_ids=true | all-gather | bytes 663552 | tf_op jit(solution)/shard_map/all_gather | solution.py:364
  61.8 3.2 %shard_map.194 = bf16[8,288,128]{2,1,0:T(8,128)(2,1)} custom-call(s32[2]{0:T(128)S(1)} %pad_add_fusion.place_ref, f32[1,1]{1,0:T(1,128)} %bitcast.16.weight_ref, bf16[8,160,128]{2,1,0:T(8,128)(2,1)S(1)} %all-to-all-done.1.team_ref, bf16[8,288,128]{2,1,0:T(8,128)(2,1)S(1)} %bitcast.17), custom_call_target="tpu_custom_call" | custom-call | tf_op jit(solution)/shard_map/pallas_call | solution.py:365
  65.0 0.0 copy-start.4
  65.0 0.0 copy-start.7
  65.0 4.6 %all-to-all-start.2 = ((bf16[8,288,128]{2,1,0:T(8,128)(2,1)}), bf16[8,288,128]{2,1,0:T(8,128)(2,1)S(1)}, u32[]{:S(2)}, u32[]{:S(2)}) async-start(bf16[8,288,128]{2,1,0:T(8,128)(2,1)} %shard_map.194), calls=%async_computation.2 | async-start | bytes 1179648 | tf_op jit(solution)/shard_map/all_to_all | solution.py:303
  69.6 0.0 copy-done.4
  69.6 0.0 copy-done.7
  69.6 0.0 copy-start.5
  69.6 0.0 copy-start.6
  69.6 0.9 shard_map.195
  70.6 6.4 %all-to-all-done.2.parts_ref = bf16[8,288,128]{2,1,0:T(8,128)(2,1)S(1)} async-done(((bf16[8,288,128]{2,1,0:T(8,128)(2,1)}), bf16[8,288,128]{2,1,0:T(8,128)(2,1)S(1)}, u32[]{:S(2)}, u32[]{:S(2)}) %all-to-all-start.2) | async-done | bytes 589856 | tf_op jit(solution)/shard_map/all_to_all | solution.py:303
  77.0 0.0 copy-done.5
  77.0 0.0 copy-done.6
  77.0 1.0 %shard_map.196 = bf16[128,2048]{1,0:T(8,128)(2,1)S(1)} custom-call(bf16[8,288,128]{2,1,0:T(8,128)(2,1)S(1)} %all-to-all-done.2.parts_ref, f32[128,128]{1,0:T(8,128)S(1)} %get-tuple-element.26.local_ref, bf16[128,64]{1,0:T(8,128)(2,1)S(1)} %get-tuple-element.27.decayed_ref, f32[128,128]{1,0:T(8,128)S(1)} %get-tuple-element.28.gate_ref, ...), custom_call_target="tpu_custom_call" | custom-call | tf_op jit(solution)/shard_map/pallas_call | solution.py:378
  78.0 19.9 %all_to_all.20 = bf16[8,16,2048]{2,1,0:T(8,128)(2,1)S(1)} all-to-all(bf16[8,16,2048]{2,1,0:T(8,128)(2,1)S(1)} %bitcast.19), channel_id=1, replica_groups=mesh['far'=8,'pair'=2,'y'=4,'x'=4,'core'=2] {'x','core'}, dimensions={0} | all-to-all | bytes 1048576 | tf_op jit(solution)/shard_map/all_to_all | solution.py:303
  97.9 0.7 reduce_sum.12
  (1 shorter events, 0.0 us)
Async XLA Ops:
  0.0 6.6 %copy-start.11 = (bf16[32,64]{1,0:T(8,128)(2,1)S(1)}, bf16[32,64]{1,0:T(8,128)(2,1)}, u32[]{:S(2)}) copy-start(bf16[32,64]{1,0:T(8,128)(2,1)} %up_ref.1) | copy-start | bytes 12292
  0.0 20.5 %copy-start.9 = (bf16[2048,32]{0,1:T(8,128)(2,1)S(1)}, bf16[2048,32]{0,1:T(8,128)(2,1)}, u32[]{:S(2)}) copy-start(bf16[2048,32]{0,1:T(8,128)(2,1)} %param.33) | copy-start | bytes 393220
  1.6 5.0 %copy-start.10 = (f32[2048]{0:T(1024)S(1)}, f32[2048]{0:T(1024)}, u32[]{:S(2)}) copy-start(f32[2048]{0:T(1024)} %param.21) | copy-start | bytes 24580
  1.6 5.0 %copy-start.12 = (f32[64]{0:T(128)S(1)}, f32[64]{0:T(128)}, u32[]{:S(2)}) copy-start(f32[64]{0:T(128)} %param.35) | copy-start | bytes 772
  1.6 5.1 %copy-start.13 = (f32[128,1]{0,1:T(1,128)S(1)}, f32[128,1]{0,1:T(1,128)}, u32[]{:S(2)}) copy-start(f32[128,1]{0,1:T(1,128)} %param.36) | copy-start | bytes 1540
  1.6 5.1 %copy-start.14 = (f32[64]{0:T(128)S(1)}, f32[64]{0:T(128)}, u32[]{:S(2)}) copy-start(f32[64]{0:T(128)} %param.25) | copy-start | bytes 772
  1.6 5.1 %copy-start.15 = (f32[64]{0:T(128)S(1)}, f32[64]{0:T(128)}, u32[]{:S(2)}) copy-start(f32[64]{0:T(128)} %param.26) | copy-start | bytes 772
  1.6 5.1 %copy-start.16 = (f32[128]{0:T(128)S(1)}, f32[128]{0:T(128)}, u32[]{:S(2)}) copy-start(f32[128]{0:T(128)} %param.28) | copy-start | bytes 1540
  1.6 5.1 %copy-start.17 = (f32[128]{0:T(128)S(1)}, f32[128]{0:T(128)}, u32[]{:S(2)}) copy-start(f32[128]{0:T(128)} %param.37) | copy-start | bytes 1540
  1.7 18.9 %copy-start.3 = (bf16[2048,128]{1,0:T(8,128)(2,1)S(1)}, bf16[2048,128]{1,0:T(8,128)(2,1)}, u32[]{:S(2)}) copy-start(bf16[2048,128]{1,0:T(8,128)(2,1)} %lv_ref.1) | copy-start | bytes 1572868
  1.7 10.5 %all-to-all-start = ((bf16[4,16,2048]{2,1,0:T(8,128)(2,1)}), bf16[4,16,2048]{2,1,0:T(8,128)(2,1)S(1)}, u32[]{:S(2)}, u32[]{:S(2)}) async-start(bf16[4,16,2048]{2,1,0:T(8,128)(2,1)} %broadcast_in_dim.3), calls=%async_computation | async-start | bytes 524288 | tf_op jit(solution)/shard_map/all_to_all | solution.py:303
  6.6 13.9 %copy-start.2 = (bf16[2048,128]{1,0:T(8,128)(2,1)S(1)}, bf16[2048,128]{1,0:T(8,128)(2,1)}, u32[]{:S(2)}) copy-start(bf16[2048,128]{1,0:T(8,128)(2,1)} %dq_ref.1) | copy-start | bytes 1572868
  6.8 13.7 %copy-start.8 = (bf16[2048,64]{0,1:T(8,128)(2,1)S(1)}, bf16[2048,64]{0,1:T(8,128)(2,1)}, u32[]{:S(2)}) copy-start(bf16[2048,64]{0,1:T(8,128)(2,1)} %param.30) | copy-start | bytes 786436
  20.5 6.5 %copy-start.1 = (bf16[2048,128]{1,0:T(8,128)(2,1)S(1)}, bf16[2048,128]{1,0:T(8,128)(2,1)}, u32[]{:S(2)}) copy-start(bf16[2048,128]{1,0:T(8,128)(2,1)} %dv_ref.1) | copy-start | bytes 1572868
  22.7 4.3 %copy-start = (bf16[2048,128]{1,0:T(8,128)(2,1)S(1)}, bf16[2048,128]{1,0:T(8,128)(2,1)}, u32[]{:S(2)}) copy-start(bf16[2048,128]{1,0:T(8,128)(2,1)} %dk_ref.1) | copy-start | bytes 1572868
  22.7 10.0 %all-to-all-start.1 = ((bf16[8,160,128]{2,1,0:T(8,128)(2,1)}), bf16[8,160,128]{2,1,0:T(8,128)(2,1)S(1)}, u32[]{:S(2)}, u32[]{:S(2)}) async-start(bf16[8,160,128]{2,1,0:T(8,128)(2,1)} %get-tuple-element.21), calls=%async_computation.1 | async-start | bytes 655360 | tf_op jit(solution)/shard_map/all_to_all | solution.py:303
  65.0 4.6 %copy-start.4 = (bf16[2048,128]{1,0:T(8,128)(2,1)S(1)}, bf16[2048,128]{1,0:T(8,128)(2,1)}, u32[]{:S(2)}) copy-start(bf16[2048,128]{1,0:T(8,128)(2,1)} %lg_ref.1) | copy-start | bytes 1572868
  65.0 4.6 %copy-start.7 = (bf16[2048,64]{0,1:T(8,128)(2,1)S(1)}, bf16[2048,64]{0,1:T(8,128)(2,1)}, u32[]{:S(2)}) copy-start(bf16[2048,64]{0,1:T(8,128)(2,1)} %param.29) | copy-start | bytes 786436
  65.0 12.0 %all-to-all-start.2 = ((bf16[8,288,128]{2,1,0:T(8,128)(2,1)}), bf16[8,288,128]{2,1,0:T(8,128)(2,1)S(1)}, u32[]{:S(2)}, u32[]{:S(2)}) async-start(bf16[8,288,128]{2,1,0:T(8,128)(2,1)} %shard_map.194), calls=%async_computation.2 | async-start | bytes 1179648 | tf_op jit(solution)/shard_map/all_to_all | solution.py:303
  69.6 7.4 %copy-start.5 = (bf16[128,2048]{1,0:T(8,128)(2,1)S(1)}, bf16[128,2048]{1,0:T(8,128)(2,1)}, u32[]{:S(2)}) copy-start(bf16[128,2048]{1,0:T(8,128)(2,1)} %drows_ref.1) | copy-start | bytes 1572868
  69.6 7.4 %copy-start.6 = (bf16[128,2048]{1,0:T(8,128)(2,1)S(1)}, bf16[128,2048]{1,0:T(8,128)(2,1)}, u32[]{:S(2)}) copy-start(bf16[128,2048]{1,0:T(8,128)(2,1)} %lrows_ref.1) | copy-start | bytes 1572868

commit v3 on v2

--- a/solution.py
+++ b/solution.py
@@ -112,20 +112,17 @@
         ).astype(BF16)
 
 
-def key_value_kernel(normed_ref, dk_ref, dv_ref, small_ref, kv_ref):
+def local_kernel(
+    normed_ref, dk_ref, dv_ref, lg_ref, lq_ref, lk_ref, lv_ref, total_ref, small_ref,
+    kv_ref, local_ref, decayed_ref, gate_ref, scores_ref,
+):
     normed = normed_ref[...]
     key = two_map_norm(dot(normed, dk_ref[...]).astype(BF16).astype(F32), small_ref[1:2])
     kv_ref[0:BLOCK] = key.astype(BF16)
     kv_ref[BLOCK:] = dot(normed, dv_ref[...]).astype(BF16)
-
-
-def local_kernel(
-    normed_ref, lg_ref, lq_ref, lk_ref, lv_ref, total_ref, local_ref, decayed_ref, gate_ref,
-    scores_ref,
-):
-    gate = dot(normed_ref[...], lg_ref[...]).astype(BF16).astype(F32)
+    gate = dot(normed, lg_ref[...]).astype(BF16).astype(F32)
     gate_ref[...] = gate * jax.nn.sigmoid(gate)
-    lq = dot_nt(normed_ref[...], lq_ref[...]).astype(BF16).astype(F32) * HEAD**-0.5
+    lq = dot_nt(normed, lq_ref[...]).astype(BF16).astype(F32) * HEAD**-0.5
     lk = lk_ref[...].astype(F32)
     lv = lv_ref[...]
     total = total_ref[...]
@@ -189,7 +186,7 @@
     def attend(blocks):
         cols, open_cols = blocks * BLOCK, (blocks - 2) * BLOCK
         last_pos = key_pos + (blocks - 2) * MEMBERS * BLOCK
-        batch = {2: 8, 4: 4}.get(blocks, 2)
+        batch = {2: 8, 4: 8, 6: 4}.get(blocks, 2)
         rows = batch * BLOCK
 
         def one(step, _):
@@ -226,7 +223,7 @@
         if batch == MEMBERS:
             one(0, 0)
         else:
-            lax.fori_loop(0, MEMBERS // batch, one, 0)
+            lax.fori_loop(0, MEMBERS // batch, one, 0, unroll=True)
 
     for blocks in range(2, GROUPS + 1, 2):
         pl.when(group // 2 == blocks // 2 - 1)(lambda blocks=blocks: attend(blocks))
@@ -346,19 +343,20 @@
         rows, gain, differential_query, linear_value, linear_key.T, forget_down_factor.T, small,
         shrunk, up,
     )
-    kv = call(key_value_kernel, shape((2 * BLOCK, VDIM), BF16), inputs=4)(
-        normed, differential_key, differential_value, small
-    )
-    local, decayed, gate = call(
+    kv, local, decayed, gate = call(
         local_kernel,
         (
+            shape((2 * BLOCK, VDIM), BF16),
             shape((BLOCK, VDIM), F32),
             shape((BLOCK, HEAD), BF16),
             shape((BLOCK, VDIM), F32),
         ),
         scratch=[pltpu.VMEM((BLOCK, BLOCK), F32)],
-        inputs=6,
-    )(normed, linear_output_gate, linear_query.T, lk, lv, total)
+        inputs=9,
+    )(
+        normed, differential_key, differential_value, linear_output_gate, linear_query.T, lk, lv,
+        total, small,
+    )
     team = exchanged(team, TEAM)
     far = call(group_kernel, shape((2 * BLOCK + 32, VDIM), BF16), inputs=2)(team, kv)
     far = lax.all_gather(far, "far")

time: 99.1 us -> 97.9 us (0.988)
  blocking collectives: 57.3 us -> 69 us
  waiting for transfers between devices: 17 us -> 9.82 us
  starting transfers between devices: 13.1 us -> 8.54 us
    all_to_all x1 -> x2, blocking collectives: 19.9 us -> 31.6 us  [exchanged(): return lax.all_to_all(blocks, axis, split_axis=0, concat_axis=0, tiled=True)]
    all_to_all x3 -> x2, waiting for transfers between devices: 17 us -> 9.82 us  [exchanged(): return lax.all_to_all(blocks, axis, split_axis=0, concat_axis=0, tiled=True)]
    all_to_all x3 -> x2, starting transfers between devices: 13.1 us -> 8.54 us  [exchanged(): return lax.all_to_all(blocks, axis, split_axis=0, concat_axis=0, tiled=True)]
  transfers between devices with their start and end apart: 3 -> 2, of which waited for: 3 -> 2; matrix products, arithmetic and copies ran while one was open for 0% -> 0% of each run, Pallas kernels for 2% -> 1%
where the time goes in v3:
time: 97.9 us; the launch traced here: 97.5 us
  blocking collectives  69 us (70%)
  waiting for transfers between devices  9.82 us (10%)
  starting transfers between devices  8.54 us (9%)
  Pallas kernels  6.91 us (7%)
  local copies, waits for them, and re-layouts  1.68 us (2%)
    all_to_all x2, blocking collectives, exchanged(): return lax.all_to_all(blocks, axis, split_axis=0, concat_axis=0, tiled=True)  31.6 us
    all_gather x1, blocking collectives, per_device(): far = lax.all_gather(far, 'far')  29 us
    all_to_all x2, waiting for transfers between devices, exchanged(): return lax.all_to_all(blocks, axis, split_axis=0, concat_axis=0, tiled=True)  9.82 us
    all_to_all x2, starting transfers between devices, exchanged(): return lax.all_to_all(blocks, axis, split_axis=0, concat_axis=0, tiled=True)  8.54 us
    all_gather x1, blocking collectives, per_device(): rows = lax.all_gather(rows, 'core')  8.33 us
    pallas_call x1, Pallas kernels, per_device(): call(attend_kernel, shape((MEMBERS, 2 * BLOCK + 32, VDIM), BF16), scratch...  2.37 us
    pallas_call x1, Pallas kernels, per_device(): call(project_kernel, (shape((MEMBERS, BLOCK + 32, VDIM), BF16), shape((BL...  2.17 us
  transfers between devices with their start and end apart: 2, of which 2 were waited for; matrix products, arithmetic and copies ran while one was open for 0% of the time, Pallas kernels for 1%

profile of v3, /device:TPU:1, one launch (start us, length us, event | category | flops | bytes accessed | tf_op | source)
XLA Modules:
  0.0 97.5 jit_solution(7452848133750778232)
XLA Ops:
  0.0 0.0 copy-start.11
  0.0 0.0 copy-start.9
  0.0 1.6 %broadcast_in_dim.3 = bf16[4,16,2048]{2,1,0:T(8,128)(2,1)} broadcast(bf16[16,2048]{1,0:T(8,128)(2,1)} %param.20), dimensions={1,2} | broadcast | bytes 327680 | tf_op jit(solution)/shard_map/broadcast_in_dim | solution.py:312
  1.6 0.0 copy-start.10
  1.6 0.0 copy-start.12
  1.6 0.0 copy-start.13
  1.6 0.0 copy-start.14
  1.6 0.0 copy-start.15
  1.6 0.0 copy-start.16
  1.6 0.0 copy-start.17
  1.6 0.0 copy-start.4
  1.7 5.0 %all-to-all-start = ((bf16[4,16,2048]{2,1,0:T(8,128)(2,1)}), bf16[4,16,2048]{2,1,0:T(8,128)(2,1)S(1)}, u32[]{:S(2)}, u32[]{:S(2)}) async-start(bf16[4,16,2048]{2,1,0:T(8,128)(2,1)} %broadcast_in_dim.3), calls=%async_computation | async-start | bytes 524288 | tf_op jit(solution)/shard_map/all_to_all | solution.py:300
  6.6 0.0 copy-start.3
  6.6 0.0 copy-done.11
  6.6 0.0 copy-done.10
  6.6 0.0 copy-done.12
  6.6 0.0 copy-done.13
  6.7 0.0 copy-done.14
  6.7 0.0 copy-done.15
  6.7 0.0 copy-done.16
  6.7 0.0 copy-done.17
  6.7 0.1 shard_map.190
  6.8 0.0 copy-start.8
  6.8 5.3 %all-to-all-done = bf16[4,16,2048]{2,1,0:T(8,128)(2,1)S(1)} async-done(((bf16[4,16,2048]{2,1,0:T(8,128)(2,1)}), bf16[4,16,2048]{2,1,0:T(8,128)(2,1)S(1)}, u32[]{:S(2)}, u32[]{:S(2)}) %all-to-all-start) | async-done | bytes 262176 | tf_op jit(solution)/shard_map/all_to_all | solution.py:300
  12.2 8.3 %all-gather = bf16[8,16,2048]{2,1,0:T(8,128)(2,1)S(1)} all-gather(bf16[4,16,2048]{2,1,0:T(8,128)(2,1)S(1)} %all-to-all-done), channel_id=2, replica_groups=mesh['far'=8,'pair'=2,'y'=4,'x'=4,'core'=2] {'core'}, dimensions={0}, use_global_device_ids=true | all-gather | bytes 786432 | tf_op jit(solution)/shard_map/all_gather | solution.py:313
  20.5 0.0 copy-done.9
  20.5 0.0 copy-done.4
  20.5 0.0 copy-done.3
  20.5 0.0 copy-done.8
  20.5 0.0 copy-start.1
  20.5 0.0 copy-start.2
  20.5 0.0 copy-start.7
  20.5 2.2 %shard_map.191 = (bf16[8,160,128]{2,1,0:T(8,128)(2,1)}, bf16[128,2048]{1,0:T(8,128)(2,1)S(1)}, bf16[128,64]{1,0:T(8,128)(2,1)S(1)}, bf16[128,128]{1,0:T(8,128)(2,1)S(1)}, f32[128,64]{1,0:T(8,128)S(1)}) custom-call(bf16[2,4,16,2048]{3,2,1,0:T(8,128)(2,1)S(1)} %bitcast.18, f32[1,2048]{1,0:T(1,128)S(1)} %get-tuple-element.18.gain_ref, ...), custom_call_target="tpu_custom_call" | custom-call | tf_op jit(solution)/shard_map/pallas_call | solution.py:332
  22.7 0.0 copy-start
  22.7 3.6 %all-to-all-start.1 = ((bf16[8,160,128]{2,1,0:T(8,128)(2,1)}), bf16[8,160,128]{2,1,0:T(8,128)(2,1)S(1)}, u32[]{:S(2)}, u32[]{:S(2)}) async-start(bf16[8,160,128]{2,1,0:T(8,128)(2,1)} %get-tuple-element.22), calls=%async_computation.1 | async-start | bytes 655360 | tf_op jit(solution)/shard_map/all_to_all | solution.py:300
  26.9 0.1 pad_add_fusion.place_ref
  27.0 0.0 copy-done.1
  27.0 0.0 copy-done.2
  27.0 0.0 copy-done.7
  27.0 0.0 copy-done
  27.0 1.2 %shard_map.192 = (bf16[256,128]{1,0:T(8,128)(2,1)S(1)}, f32[128,128]{1,0:T(8,128)S(1)}, bf16[128,64]{1,0:T(8,128)(2,1)S(1)}, f32[128,128]{1,0:T(8,128)S(1)}) custom-call(bf16[128,2048]{1,0:T(8,128)(2,1)S(1)} %get-tuple-element.23.normed_ref, bf16[2048,128]{1,0:T(8,128)(2,1)S(1)} %copy-done, bf16[2048,128]{1,0:T(8,128)(2,1)S(1)} %copy-done.1, ...), custom_call_target="tpu_custom_call" | custom-call | tf_op jit(solution)/shard_map/pallas_call | solution.py:346
  28.2 4.5 %all-to-all-done.1.team_ref = bf16[8,160,128]{2,1,0:T(8,128)(2,1)S(1)} async-done(((bf16[8,160,128]{2,1,0:T(8,128)(2,1)}), bf16[8,160,128]{2,1,0:T(8,128)(2,1)S(1)}, u32[]{:S(2)}, u32[]{:S(2)}) %all-to-all-start.1) | async-done | bytes 327712 | tf_op jit(solution)/shard_map/all_to_all | solution.py:300
  32.8 29.0 %all-gather.1 = bf16[2304,128]{1,0:T(8,128)(2,1)S(1)} all-gather(bf16[288,128]{1,0:T(8,128)(2,1)S(1)} %shard_map.193), channel_id=3, replica_groups=mesh['far'=8,'pair'=2,'y'=4,'x'=4,'core'=2] {'far'}, dimensions={0}, use_global_device_ids=true | all-gather | bytes 663552 | tf_op jit(solution)/shard_map/all_gather | solution.py:362
  61.8 2.4 %shard_map.194 = bf16[8,288,128]{2,1,0:T(8,128)(2,1)S(1)} custom-call(s32[2]{0:T(128)S(1)} %pad_add_fusion.place_ref, f32[1,1]{1,0:T(1,128)} %bitcast.16.weight_ref, bf16[8,160,128]{2,1,0:T(8,128)(2,1)S(1)} %all-to-all-done.1.team_ref, bf16[8,288,128]{2,1,0:T(8,128)(2,1)S(1)} %bitcast.17), custom_call_target="tpu_custom_call" | custom-call | tf_op jit(solution)/shard_map/pallas_call | solution.py:363
  64.2 0.0 copy-start.5
  64.2 0.0 copy-start.6
  64.2 12.4 %all_to_all.20.parts_ref = bf16[8,288,128]{2,1,0:T(8,128)(2,1)S(1)} all-to-all(bf16[8,288,128]{2,1,0:T(8,128)(2,1)S(1)} %shard_map.194), channel_id=1, replica_groups=mesh['far'=8,'pair'=2,'y'=4,'x'=4,'core'=2] {'pair','y'}, dimensions={0} | all-to-all | bytes 1179648 | tf_op jit(solution)/shard_map/all_to_all | solution.py:300
  76.6 0.0 copy-done.5
  76.6 0.0 copy-done.6
  76.6 1.0 %shard_map.195 = bf16[128,2048]{1,0:T(8,128)(2,1)S(1)} custom-call(bf16[8,288,128]{2,1,0:T(8,128)(2,1)S(1)} %all_to_all.20.parts_ref, f32[128,128]{1,0:T(8,128)S(1)} %get-tuple-element.28.local_ref, bf16[128,64]{1,0:T(8,128)(2,1)S(1)} %get-tuple-element.29.decayed_ref, f32[128,128]{1,0:T(8,128)S(1)} %get-tuple-element.30.gate_ref, ...), custom_call_target="tpu_custom_call" | custom-call | tf_op jit(solution)/shard_map/pallas_call | solution.py:376
  77.6 19.2 %all_to_all.21 = bf16[8,16,2048]{2,1,0:T(8,128)(2,1)S(1)} all-to-all(bf16[8,16,2048]{2,1,0:T(8,128)(2,1)S(1)} %bitcast.19), channel_id=1, replica_groups=mesh['far'=8,'pair'=2,'y'=4,'x'=4,'core'=2] {'x','core'}, dimensions={0} | all-to-all | bytes 1048576 | tf_op jit(solution)/shard_map/all_to_all | solution.py:300
  96.8 0.7 reduce_sum.12
  (1 shorter events, 0.0 us)
Async XLA Ops:
  0.0 6.6 %copy-start.11 = (bf16[32,64]{1,0:T(8,128)(2,1)S(1)}, bf16[32,64]{1,0:T(8,128)(2,1)}, u32[]{:S(2)}) copy-start(bf16[32,64]{1,0:T(8,128)(2,1)} %up_ref.1) | copy-start | bytes 12292
  0.0 20.5 %copy-start.9 = (bf16[2048,32]{0,1:T(8,128)(2,1)S(1)}, bf16[2048,32]{0,1:T(8,128)(2,1)}, u32[]{:S(2)}) copy-start(bf16[2048,32]{0,1:T(8,128)(2,1)} %param.33) | copy-start | bytes 393220
  1.6 5.0 %copy-start.10 = (f32[2048]{0:T(1024)S(1)}, f32[2048]{0:T(1024)}, u32[]{:S(2)}) copy-start(f32[2048]{0:T(1024)} %param.21) | copy-start | bytes 24580
  1.6 5.0 %copy-start.12 = (f32[64]{0:T(128)S(1)}, f32[64]{0:T(128)}, u32[]{:S(2)}) copy-start(f32[64]{0:T(128)} %param.35) | copy-start | bytes 772
  1.6 5.1 %copy-start.13 = (f32[128,1]{0,1:T(1,128)S(1)}, f32[128,1]{0,1:T(1,128)}, u32[]{:S(2)}) copy-start(f32[128,1]{0,1:T(1,128)} %param.36) | copy-start | bytes 1540
  1.6 5.1 %copy-start.14 = (f32[64]{0:T(128)S(1)}, f32[64]{0:T(128)}, u32[]{:S(2)}) copy-start(f32[64]{0:T(128)} %param.25) | copy-start | bytes 772
  1.6 5.1 %copy-start.15 = (f32[64]{0:T(128)S(1)}, f32[64]{0:T(128)}, u32[]{:S(2)}) copy-start(f32[64]{0:T(128)} %param.26) | copy-start | bytes 772
  1.6 5.1 %copy-start.16 = (f32[128]{0:T(128)S(1)}, f32[128]{0:T(128)}, u32[]{:S(2)}) copy-start(f32[128]{0:T(128)} %param.28) | copy-start | bytes 1540
  1.6 5.1 %copy-start.17 = (f32[128]{0:T(128)S(1)}, f32[128]{0:T(128)}, u32[]{:S(2)}) copy-start(f32[128]{0:T(128)} %param.37) | copy-start | bytes 1540
  1.6 18.9 %copy-start.4 = (bf16[2048,128]{1,0:T(8,128)(2,1)S(1)}, bf16[2048,128]{1,0:T(8,128)(2,1)}, u32[]{:S(2)}) copy-start(bf16[2048,128]{1,0:T(8,128)(2,1)} %lv_ref.1) | copy-start | bytes 1572868
  1.7 10.5 %all-to-all-start = ((bf16[4,16,2048]{2,1,0:T(8,128)(2,1)}), bf16[4,16,2048]{2,1,0:T(8,128)(2,1)S(1)}, u32[]{:S(2)}, u32[]{:S(2)}) async-start(bf16[4,16,2048]{2,1,0:T(8,128)(2,1)} %broadcast_in_dim.3), calls=%async_computation | async-start | bytes 524288 | tf_op jit(solution)/shard_map/all_to_all | solution.py:300
  6.6 13.9 %copy-start.3 = (bf16[2048,128]{1,0:T(8,128)(2,1)S(1)}, bf16[2048,128]{1,0:T(8,128)(2,1)}, u32[]{:S(2)}) copy-start(bf16[2048,128]{1,0:T(8,128)(2,1)} %dq_ref.1) | copy-start | bytes 1572868
  6.8 13.7 %copy-start.8 = (bf16[2048,64]{0,1:T(8,128)(2,1)S(1)}, bf16[2048,64]{0,1:T(8,128)(2,1)}, u32[]{:S(2)}) copy-start(bf16[2048,64]{0,1:T(8,128)(2,1)} %param.30) | copy-start | bytes 786436
  20.5 6.5 %copy-start.1 = (bf16[2048,128]{1,0:T(8,128)(2,1)S(1)}, bf16[2048,128]{1,0:T(8,128)(2,1)}, u32[]{:S(2)}) copy-start(bf16[2048,128]{1,0:T(8,128)(2,1)} %dv_ref.1) | copy-start | bytes 1572868
  20.5 6.5 %copy-start.2 = (bf16[2048,128]{1,0:T(8,128)(2,1)S(1)}, bf16[2048,128]{1,0:T(8,128)(2,1)}, u32[]{:S(2)}) copy-start(bf16[2048,128]{1,0:T(8,128)(2,1)} %lg_ref.1) | copy-start | bytes 1572868
  20.5 6.5 %copy-start.7 = (bf16[2048,64]{0,1:T(8,128)(2,1)S(1)}, bf16[2048,64]{0,1:T(8,128)(2,1)}, u32[]{:S(2)}) copy-start(bf16[2048,64]{0,1:T(8,128)(2,1)} %param.29) | copy-start | bytes 786436
  22.7 4.3 %copy-start = (bf16[2048,128]{1,0:T(8,128)(2,1)S(1)}, bf16[2048,128]{1,0:T(8,128)(2,1)}, u32[]{:S(2)}) copy-start(bf16[2048,128]{1,0:T(8,128)(2,1)} %dk_ref.1) | copy-start | bytes 1572868
  22.7 10.0 %all-to-all-start.1 = ((bf16[8,160,128]{2,1,0:T(8,128)(2,1)}), bf16[8,160,128]{2,1,0:T(8,128)(2,1)S(1)}, u32[]{:S(2)}, u32[]{:S(2)}) async-start(bf16[8,160,128]{2,1,0:T(8,128)(2,1)} %get-tuple-element.22), calls=%async_computation.1 | async-start | bytes 655360 | tf_op jit(solution)/shard_map/all_to_all | solution.py:300
  64.2 12.4 %copy-start.5 = (bf16[128,2048]{1,0:T(8,128)(2,1)S(1)}, bf16[128,2048]{1,0:T(8,128)(2,1)}, u32[]{:S(2)}) copy-start(bf16[128,2048]{1,0:T(8,128)(2,1)} %drows_ref.1) | copy-start | bytes 1572868
  64.2 12.4 %copy-start.6 = (bf16[128,2048]{1,0:T(8,128)(2,1)S(1)}, bf16[128,2048]{1,0:T(8,128)(2,1)}, u32[]{:S(2)}) copy-start(bf16[128,2048]{1,0:T(8,128)(2,1)} %lrows_ref.1) | copy-start | bytes 1572868

commit v4 on v3

--- a/solution.py
+++ b/solution.py
@@ -69,6 +69,12 @@
     shrunk_ref[...] = jnp.broadcast_to(shrink_ref[...], shrunk_ref.shape).T
     ready_gain_ref[...] = gain_ref[...]
     ready_up_ref[...] = up_ref[...]
+
+
+def copy_kernel(tokens_ref, copies_ref):
+    tokens = tokens_ref[...]
+    for chip in range(copies_ref.shape[0]):
+        copies_ref[chip] = tokens
 
 
 def project_kernel(
@@ -309,7 +315,8 @@
 ):
     shape = jax.ShapeDtypeStruct
     copies = lax.axis_size(TP)
-    rows = exchanged(jnp.broadcast_to(tokens, (copies // 2, *tokens.shape)), "x")
+    rows = call(copy_kernel, shape((copies // 2, *tokens.shape), BF16), inputs=1)(tokens)
+    rows = exchanged(rows, "x")
     rows = lax.all_gather(rows, "core")
     place = jnp.stack([lax.axis_index("far"), lax.axis_index(TEAM)]).astype(jnp.int32)
 

time: 97.9 us -> 97.9 us (level)
    broadcast_in_dim x1 -> x0, local copies, waits for them, and re-layouts: 1.59 us -> none  [per_device(): jnp.broadcast_to(tokens, (copies // 2, *tokens.shape))]
where the time goes in v4:
time: 97.9 us; the launch traced here: 97.5 us
  blocking collectives  69 us (70%)
  waiting for transfers between devices  9.81 us (10%)
  starting transfers between devices  8.54 us (9%)
  Pallas kernels  7.62 us (8%)
    all_to_all x2, blocking collectives, exchanged(): return lax.all_to_all(blocks, axis, split_axis=0, concat_axis=0, tiled=True)  31.4 us
    all_gather x1, blocking collectives, per_device(): far = lax.all_gather(far, 'far')  29.2 us
    all_to_all x2, waiting for transfers between devices, exchanged(): return lax.all_to_all(blocks, axis, split_axis=0, concat_axis=0, tiled=True)  9.81 us
    all_to_all x2, starting transfers between devices, exchanged(): return lax.all_to_all(blocks, axis, split_axis=0, concat_axis=0, tiled=True)  8.54 us
    all_gather x1, blocking collectives, per_device(): rows = lax.all_gather(rows, 'core')  8.33 us
    pallas_call x1, Pallas kernels, per_device(): call(attend_kernel, shape((MEMBERS, 2 * BLOCK + 32, VDIM), BF16), scratch...  2.37 us
    pallas_call x1, Pallas kernels, per_device(): call(project_kernel, (shape((MEMBERS, BLOCK + 32, VDIM), BF16), shape((BL...  2.16 us
  transfers between devices with their start and end apart: 2, of which 2 were waited for; matrix products, arithmetic and copies ran while one was open for 0% of the time, Pallas kernels for 1%

profile of v4, /device:TPU:1, one launch (start us, length us, event | category | flops | bytes accessed | tf_op | source)
XLA Modules:
  0.0 97.5 jit_solution(259609555244735103)
XLA Ops:
  0.0 0.0 copy-start.10
  0.0 0.8 copy-done.10
  0.8 0.0 copy-start.12
  0.8 0.0 copy-start.9
  0.8 0.7 shard_map.190
  1.6 0.0 copy-start.11
  1.6 0.0 copy-start.13
  1.6 0.0 copy-start.14
  1.6 0.0 copy-start.15
  1.6 0.0 copy-start.16
  1.6 0.0 copy-start.17
  1.6 0.0 copy-start.18
  1.6 0.0 copy-start.4
  1.6 5.0 %all-to-all-start = ((bf16[4,16,2048]{2,1,0:T(8,128)(2,1)}), bf16[4,16,2048]{2,1,0:T(8,128)(2,1)S(1)}, u32[]{:S(2)}, u32[]{:S(2)}) async-start(bf16[4,16,2048]{2,1,0:T(8,128)(2,1)} %shard_map.190), calls=%async_computation | async-start | bytes 524288 | tf_op jit(solution)/shard_map/all_to_all | solution.py:306
  6.6 0.0 copy-start.3
  6.6 0.0 copy-done.12
  6.6 0.0 copy-done.11
  6.6 0.0 copy-done.13
  6.6 0.0 copy-done.14
  6.6 0.0 copy-done.15
  6.6 0.0 copy-done.16
  6.6 0.0 copy-done.17
  6.7 0.0 copy-done.18
  6.7 0.1 shard_map.191
  6.8 0.0 copy-start.8
  6.8 5.3 %all-to-all-done = bf16[4,16,2048]{2,1,0:T(8,128)(2,1)S(1)} async-done(((bf16[4,16,2048]{2,1,0:T(8,128)(2,1)}), bf16[4,16,2048]{2,1,0:T(8,128)(2,1)S(1)}, u32[]{:S(2)}, u32[]{:S(2)}) %all-to-all-start) | async-done | bytes 262176 | tf_op jit(solution)/shard_map/all_to_all | solution.py:306
  12.1 8.3 %all-gather = bf16[8,16,2048]{2,1,0:T(8,128)(2,1)S(1)} all-gather(bf16[4,16,2048]{2,1,0:T(8,128)(2,1)S(1)} %all-to-all-done), channel_id=2, replica_groups=mesh['far'=8,'pair'=2,'y'=4,'x'=4,'core'=2] {'core'}, dimensions={0}, use_global_device_ids=true | all-gather | bytes 786432 | tf_op jit(solution)/shard_map/all_gather | solution.py:320
  20.5 0.0 copy-done.9
  20.5 0.0 copy-done.4
  20.5 0.0 copy-done.3
  20.5 0.0 copy-done.8
  20.5 0.0 copy-start.1
  20.5 0.0 copy-start.2
  20.5 0.0 copy-start.7
  20.5 2.2 %shard_map.192 = (bf16[8,160,128]{2,1,0:T(8,128)(2,1)}, bf16[128,2048]{1,0:T(8,128)(2,1)S(1)}, bf16[128,64]{1,0:T(8,128)(2,1)S(1)}, bf16[128,128]{1,0:T(8,128)(2,1)S(1)}, f32[128,64]{1,0:T(8,128)S(1)}) custom-call(bf16[2,4,16,2048]{3,2,1,0:T(8,128)(2,1)S(1)} %bitcast.18, f32[1,2048]{1,0:T(1,128)S(1)} %get-tuple-element.18.gain_ref, ...), custom_call_target="tpu_custom_call" | custom-call | tf_op jit(solution)/shard_map/pallas_call | solution.py:339
  22.7 0.0 copy-start
  22.7 3.6 %all-to-all-start.1 = ((bf16[8,160,128]{2,1,0:T(8,128)(2,1)}), bf16[8,160,128]{2,1,0:T(8,128)(2,1)S(1)}, u32[]{:S(2)}, u32[]{:S(2)}) async-start(bf16[8,160,128]{2,1,0:T(8,128)(2,1)} %get-tuple-element.22), calls=%async_computation.1 | async-start | bytes 655360 | tf_op jit(solution)/shard_map/all_to_all | solution.py:306
  26.9 0.1 pad_add_fusion.place_ref
  27.0 0.0 copy-done.1
  27.0 0.0 copy-done.2
  27.0 0.0 copy-done.7
  27.0 0.0 copy-done
  27.0 1.2 %shard_map.193 = (bf16[256,128]{1,0:T(8,128)(2,1)S(1)}, f32[128,128]{1,0:T(8,128)S(1)}, bf16[128,64]{1,0:T(8,128)(2,1)S(1)}, f32[128,128]{1,0:T(8,128)S(1)}) custom-call(bf16[128,2048]{1,0:T(8,128)(2,1)S(1)} %get-tuple-element.23.normed_ref, bf16[2048,128]{1,0:T(8,128)(2,1)S(1)} %copy-done, bf16[2048,128]{1,0:T(8,128)(2,1)S(1)} %copy-done.1, ...), custom_call_target="tpu_custom_call" | custom-call | tf_op jit(solution)/shard_map/pallas_call | solution.py:353
  28.2 4.5 %all-to-all-done.1.team_ref = bf16[8,160,128]{2,1,0:T(8,128)(2,1)S(1)} async-done(((bf16[8,160,128]{2,1,0:T(8,128)(2,1)}), bf16[8,160,128]{2,1,0:T(8,128)(2,1)S(1)}, u32[]{:S(2)}, u32[]{:S(2)}) %all-to-all-start.1) | async-done | bytes 327712 | tf_op jit(solution)/shard_map/all_to_all | solution.py:306
  32.7 29.2 %all-gather.1 = bf16[2304,128]{1,0:T(8,128)(2,1)S(1)} all-gather(bf16[288,128]{1,0:T(8,128)(2,1)S(1)} %shard_map.194), channel_id=3, replica_groups=mesh['far'=8,'pair'=2,'y'=4,'x'=4,'core'=2] {'far'}, dimensions={0}, use_global_device_ids=true | all-gather | bytes 663552 | tf_op jit(solution)/shard_map/all_gather | solution.py:369
  61.9 2.4 %shard_map.195 = bf16[8,288,128]{2,1,0:T(8,128)(2,1)S(1)} custom-call(s32[2]{0:T(128)S(1)} %pad_add_fusion.place_ref, f32[1,1]{1,0:T(1,128)} %bitcast.16.weight_ref, bf16[8,160,128]{2,1,0:T(8,128)(2,1)S(1)} %all-to-all-done.1.team_ref, bf16[8,288,128]{2,1,0:T(8,128)(2,1)S(1)} %bitcast.17), custom_call_target="tpu_custom_call" | custom-call | tf_op jit(solution)/shard_map/pallas_call | solution.py:370
  64.3 0.0 copy-start.5
  64.3 0.0 copy-start.6
  64.3 11.5 %all_to_all.20.parts_ref = bf16[8,288,128]{2,1,0:T(8,128)(2,1)S(1)} all-to-all(bf16[8,288,128]{2,1,0:T(8,128)(2,1)S(1)} %shard_map.195), channel_id=1, replica_groups=mesh['far'=8,'pair'=2,'y'=4,'x'=4,'core'=2] {'pair','y'}, dimensions={0} | all-to-all | bytes 1179648 | tf_op jit(solution)/shard_map/all_to_all | solution.py:306
  75.9 0.0 copy-done.5
  75.9 0.0 copy-done.6
  75.9 1.0 %shard_map.196 = bf16[128,2048]{1,0:T(8,128)(2,1)S(1)} custom-call(bf16[8,288,128]{2,1,0:T(8,128)(2,1)S(1)} %all_to_all.20.parts_ref, f32[128,128]{1,0:T(8,128)S(1)} %get-tuple-element.28.local_ref, bf16[128,64]{1,0:T(8,128)(2,1)S(1)} %get-tuple-element.29.decayed_ref, f32[128,128]{1,0:T(8,128)S(1)} %get-tuple-element.30.gate_ref, ...), custom_call_target="tpu_custom_call" | custom-call | tf_op jit(solution)/shard_map/pallas_call | solution.py:383
  76.9 19.9 %all_to_all.21 = bf16[8,16,2048]{2,1,0:T(8,128)(2,1)S(1)} all-to-all(bf16[8,16,2048]{2,1,0:T(8,128)(2,1)S(1)} %bitcast.19), channel_id=1, replica_groups=mesh['far'=8,'pair'=2,'y'=4,'x'=4,'core'=2] {'x','core'}, dimensions={0} | all-to-all | bytes 1048576 | tf_op jit(solution)/shard_map/all_to_all | solution.py:306
  96.8 0.7 reduce_sum.12
  (1 shorter events, 0.0 us)
Async XLA Ops:
  0.0 0.8 copy-start.10
  0.8 5.8 %copy-start.12 = (bf16[32,64]{1,0:T(8,128)(2,1)S(1)}, bf16[32,64]{1,0:T(8,128)(2,1)}, u32[]{:S(2)}) copy-start(bf16[32,64]{1,0:T(8,128)(2,1)} %up_ref.1) | copy-start | bytes 12292
  0.8 19.6 %copy-start.9 = (bf16[2048,32]{0,1:T(8,128)(2,1)S(1)}, bf16[2048,32]{0,1:T(8,128)(2,1)}, u32[]{:S(2)}) copy-start(bf16[2048,32]{0,1:T(8,128)(2,1)} %param.33) | copy-start | bytes 393220
  1.6 5.0 %copy-start.11 = (f32[2048]{0:T(1024)S(1)}, f32[2048]{0:T(1024)}, u32[]{:S(2)}) copy-start(f32[2048]{0:T(1024)} %param.21) | copy-start | bytes 24580
  1.6 5.0 %copy-start.13 = (f32[64]{0:T(128)S(1)}, f32[64]{0:T(128)}, u32[]{:S(2)}) copy-start(f32[64]{0:T(128)} %param.35) | copy-start | bytes 772
  1.6 5.1 %copy-start.14 = (f32[128,1]{0,1:T(1,128)S(1)}, f32[128,1]{0,1:T(1,128)}, u32[]{:S(2)}) copy-start(f32[128,1]{0,1:T(1,128)} %param.36) | copy-start | bytes 1540
  1.6 5.1 %copy-start.15 = (f32[64]{0:T(128)S(1)}, f32[64]{0:T(128)}, u32[]{:S(2)}) copy-start(f32[64]{0:T(128)} %param.25) | copy-start | bytes 772
  1.6 5.1 %copy-start.16 = (f32[64]{0:T(128)S(1)}, f32[64]{0:T(128)}, u32[]{:S(2)}) copy-start(f32[64]{0:T(128)} %param.26) | copy-start | bytes 772
  1.6 5.1 %copy-start.17 = (f32[128]{0:T(128)S(1)}, f32[128]{0:T(128)}, u32[]{:S(2)}) copy-start(f32[128]{0:T(128)} %param.28) | copy-start | bytes 1540
  1.6 5.1 %copy-start.18 = (f32[128]{0:T(128)S(1)}, f32[128]{0:T(128)}, u32[]{:S(2)}) copy-start(f32[128]{0:T(128)} %param.37) | copy-start | bytes 1540
  1.6 18.9 %copy-start.4 = (bf16[2048,128]{1,0:T(8,128)(2,1)S(1)}, bf16[2048,128]{1,0:T(8,128)(2,1)}, u32[]{:S(2)}) copy-start(bf16[2048,128]{1,0:T(8,128)(2,1)} %lv_ref.1) | copy-start | bytes 1572868
  1.6 10.5 %all-to-all-start = ((bf16[4,16,2048]{2,1,0:T(8,128)(2,1)}), bf16[4,16,2048]{2,1,0:T(8,128)(2,1)S(1)}, u32[]{:S(2)}, u32[]{:S(2)}) async-start(bf16[4,16,2048]{2,1,0:T(8,128)(2,1)} %shard_map.190), calls=%async_computation | async-start | bytes 524288 | tf_op jit(solution)/shard_map/all_to_all | solution.py:306
  6.6 13.9 %copy-start.3 = (bf16[2048,128]{1,0:T(8,128)(2,1)S(1)}, bf16[2048,128]{1,0:T(8,128)(2,1)}, u32[]{:S(2)}) copy-start(bf16[2048,128]{1,0:T(8,128)(2,1)} %dq_ref.1) | copy-start | bytes 1572868
  6.8 13.7 %copy-start.8 = (bf16[2048,64]{0,1:T(8,128)(2,1)S(1)}, bf16[2048,64]{0,1:T(8,128)(2,1)}, u32[]{:S(2)}) copy-start(bf16[2048,64]{0,1:T(8,128)(2,1)} %param.30) | copy-start | bytes 786436
  20.5 6.5 %copy-start.1 = (bf16[2048,128]{1,0:T(8,128)(2,1)S(1)}, bf16[2048,128]{1,0:T(8,128)(2,1)}, u32[]{:S(2)}) copy-start(bf16[2048,128]{1,0:T(8,128)(2,1)} %dv_ref.1) | copy-start | bytes 1572868
  20.5 6.5 %copy-start.2 = (bf16[2048,128]{1,0:T(8,128)(2,1)S(1)}, bf16[2048,128]{1,0:T(8,128)(2,1)}, u32[]{:S(2)}) copy-start(bf16[2048,128]{1,0:T(8,128)(2,1)} %lg_ref.1) | copy-start | bytes 1572868
  20.5 6.5 %copy-start.7 = (bf16[2048,64]{0,1:T(8,128)(2,1)S(1)}, bf16[2048,64]{0,1:T(8,128)(2,1)}, u32[]{:S(2)}) copy-start(bf16[2048,64]{0,1:T(8,128)(2,1)} %param.29) | copy-start | bytes 786436
  22.7 4.3 %copy-start = (bf16[2048,128]{1,0:T(8,128)(2,1)S(1)}, bf16[2048,128]{1,0:T(8,128)(2,1)}, u32[]{:S(2)}) copy-start(bf16[2048,128]{1,0:T(8,128)(2,1)} %dk_ref.1) | copy-start | bytes 1572868
  22.7 10.0 %all-to-all-start.1 = ((bf16[8,160,128]{2,1,0:T(8,128)(2,1)}), bf16[8,160,128]{2,1,0:T(8,128)(2,1)S(1)}, u32[]{:S(2)}, u32[]{:S(2)}) async-start(bf16[8,160,128]{2,1,0:T(8,128)(2,1)} %get-tuple-element.22), calls=%async_computation.1 | async-start | bytes 655360 | tf_op jit(solution)/shard_map/all_to_all | solution.py:306
  64.3 11.6 %copy-start.5 = (bf16[128,2048]{1,0:T(8,128)(2,1)S(1)}, bf16[128,2048]{1,0:T(8,128)(2,1)}, u32[]{:S(2)}) copy-start(bf16[128,2048]{1,0:T(8,128)(2,1)} %drows_ref.1) | copy-start | bytes 1572868
  64.3 11.6 %copy-start.6 = (bf16[128,2048]{1,0:T(8,128)(2,1)S(1)}, bf16[128,2048]{1,0:T(8,128)(2,1)}, u32[]{:S(2)}) copy-start(bf16[128,2048]{1,0:T(8,128)(2,1)} %lrows_ref.1) | copy-start | bytes 1572868

commit v5 on v4

--- a/solution.py
+++ b/solution.py
@@ -245,8 +245,7 @@
     for index in range(MEMBERS):
         pair = slice(2 * index, 2 * index + 2)
         tail = jnp.concatenate(
-            [part[pair] for part in log_parts]
-            + [jnp.zeros((10, VDIM), F32), *two_parts(carried)],
+            [part[pair] for part in log_parts] + [jnp.zeros((2, VDIM), F32), carried],
             axis=0,
         )
         out_ref[index, 2 * BLOCK :] = tail.astype(BF16)
@@ -264,7 +263,7 @@
             logs[which].append(
                 tail[which : which + 1] + tail[which + 2 : which + 3] + tail[which + 4 : which + 5]
             )
-        states.append(tail[16:24] + tail[24:32])
+        states.append(tail[8:16])
     shares = []
     for which in range(2):
         stacked = jnp.concatenate(logs[which], axis=0)
@@ -369,7 +368,7 @@
     far = lax.all_gather(far, "far")
     parts = call(
         attend_kernel,
-        shape((MEMBERS, 2 * BLOCK + 32, VDIM), BF16),
+        shape((MEMBERS, 2 * BLOCK + 16, VDIM), BF16),
         scratch=[
             pltpu.VMEM((MEMBERS * BLOCK, VDIM), BF16),
             pltpu.VMEM((GROUPS * BLOCK, VDIM), BF16),

time: 97.9 us -> 97.8 us (level)
  no operation moved by 1% of the time
where the time goes in v5:
time: 97.8 us; the launch traced here: 97.4 us
  blocking collectives  68.9 us (70%)
  waiting for transfers between devices  9.81 us (10%)
  starting transfers between devices  8.54 us (9%)
  Pallas kernels  7.62 us (8%)
    all_to_all x2, blocking collectives, exchanged(): return lax.all_to_all(blocks, axis, split_axis=0, concat_axis=0, tiled=True)  31.3 us
    all_gather x1, blocking collectives, per_device(): far = lax.all_gather(far, 'far')  29.2 us
    all_to_all x2, waiting for transfers between devices, exchanged(): return lax.all_to_all(blocks, axis, split_axis=0, concat_axis=0, tiled=True)  9.81 us
    all_to_all x2, starting transfers between devices, exchanged(): return lax.all_to_all(blocks, axis, split_axis=0, concat_axis=0, tiled=True)  8.54 us
    all_gather x1, blocking collectives, per_device(): rows = lax.all_gather(rows, 'core')  8.33 us
    pallas_call x1, Pallas kernels, per_device(): call(attend_kernel, shape((MEMBERS, 2 * BLOCK + 16, VDIM), BF16), scratch...  2.37 us
    pallas_call x1, Pallas kernels, per_device(): call(project_kernel, (shape((MEMBERS, BLOCK + 32, VDIM), BF16), shape((BL...  2.16 us
  transfers between devices with their start and end apart: 2, of which 2 were waited for; matrix products, arithmetic and copies ran while one was open for 0% of the time, Pallas kernels for 1%

profile of v5, /device:TPU:1, one launch (start us, length us, event | category | flops | bytes accessed | tf_op | source)
XLA Modules:
  0.0 97.4 jit_solution(17165026186170756313)
XLA Ops:
  0.0 0.0 copy-start.10
  0.0 0.8 copy-done.10
  0.8 0.0 copy-start.12
  0.8 0.0 copy-start.9
  0.8 0.7 shard_map.190
  1.6 0.0 copy-start.11
  1.6 0.0 copy-start.13
  1.6 0.0 copy-start.14
  1.6 0.0 copy-start.15
  1.6 0.0 copy-start.16
  1.6 0.0 copy-start.17
  1.6 0.0 copy-start.18
  1.6 0.0 copy-start.4
  1.6 5.0 %all-to-all-start = ((bf16[4,16,2048]{2,1,0:T(8,128)(2,1)}), bf16[4,16,2048]{2,1,0:T(8,128)(2,1)S(1)}, u32[]{:S(2)}, u32[]{:S(2)}) async-start(bf16[4,16,2048]{2,1,0:T(8,128)(2,1)} %shard_map.190), calls=%async_computation | async-start | bytes 524288 | tf_op jit(solution)/shard_map/all_to_all | solution.py:305
  6.6 0.0 copy-start.3
  6.6 0.0 copy-done.12
  6.6 0.0 copy-done.11
  6.6 0.0 copy-done.13
  6.6 0.0 copy-done.14
  6.6 0.0 copy-done.15
  6.6 0.0 copy-done.16
  6.6 0.0 copy-done.17
  6.7 0.0 copy-done.18
  6.7 0.1 shard_map.191
  6.8 0.0 copy-start.8
  6.8 5.3 %all-to-all-done = bf16[4,16,2048]{2,1,0:T(8,128)(2,1)S(1)} async-done(((bf16[4,16,2048]{2,1,0:T(8,128)(2,1)}), bf16[4,16,2048]{2,1,0:T(8,128)(2,1)S(1)}, u32[]{:S(2)}, u32[]{:S(2)}) %all-to-all-start) | async-done | bytes 262176 | tf_op jit(solution)/shard_map/all_to_all | solution.py:305
  12.1 8.3 %all-gather = bf16[8,16,2048]{2,1,0:T(8,128)(2,1)S(1)} all-gather(bf16[4,16,2048]{2,1,0:T(8,128)(2,1)S(1)} %all-to-all-done), channel_id=2, replica_groups=mesh['far'=8,'pair'=2,'y'=4,'x'=4,'core'=2] {'core'}, dimensions={0}, use_global_device_ids=true | all-gather | bytes 786432 | tf_op jit(solution)/shard_map/all_gather | solution.py:319
  20.5 0.0 copy-done.9
  20.5 0.0 copy-done.4
  20.5 0.0 copy-done.3
  20.5 0.0 copy-done.8
  20.5 0.0 copy-start.1
  20.5 0.0 copy-start.2
  20.5 0.0 copy-start.7
  20.5 2.2 %shard_map.192 = (bf16[8,160,128]{2,1,0:T(8,128)(2,1)}, bf16[128,2048]{1,0:T(8,128)(2,1)S(1)}, bf16[128,64]{1,0:T(8,128)(2,1)S(1)}, bf16[128,128]{1,0:T(8,128)(2,1)S(1)}, f32[128,64]{1,0:T(8,128)S(1)}) custom-call(bf16[2,4,16,2048]{3,2,1,0:T(8,128)(2,1)S(1)} %bitcast.18, f32[1,2048]{1,0:T(1,128)S(1)} %get-tuple-element.18.gain_ref, ...), custom_call_target="tpu_custom_call" | custom-call | tf_op jit(solution)/shard_map/pallas_call | solution.py:338
  22.7 0.0 copy-start
  22.7 3.6 %all-to-all-start.1 = ((bf16[8,160,128]{2,1,0:T(8,128)(2,1)}), bf16[8,160,128]{2,1,0:T(8,128)(2,1)S(1)}, u32[]{:S(2)}, u32[]{:S(2)}) async-start(bf16[8,160,128]{2,1,0:T(8,128)(2,1)} %get-tuple-element.22), calls=%async_computation.1 | async-start | bytes 655360 | tf_op jit(solution)/shard_map/all_to_all | solution.py:305
  26.9 0.1 pad_add_fusion.place_ref
  27.0 0.0 copy-done.1
  27.0 0.0 copy-done.2
  27.0 0.0 copy-done.7
  27.0 0.0 copy-done
  27.0 1.2 %shard_map.193 = (bf16[256,128]{1,0:T(8,128)(2,1)S(1)}, f32[128,128]{1,0:T(8,128)S(1)}, bf16[128,64]{1,0:T(8,128)(2,1)S(1)}, f32[128,128]{1,0:T(8,128)S(1)}) custom-call(bf16[128,2048]{1,0:T(8,128)(2,1)S(1)} %get-tuple-element.23.normed_ref, bf16[2048,128]{1,0:T(8,128)(2,1)S(1)} %copy-done, bf16[2048,128]{1,0:T(8,128)(2,1)S(1)} %copy-done.1, ...), custom_call_target="tpu_custom_call" | custom-call | tf_op jit(solution)/shard_map/pallas_call | solution.py:352
  28.2 4.5 %all-to-all-done.1.team_ref = bf16[8,160,128]{2,1,0:T(8,128)(2,1)S(1)} async-done(((bf16[8,160,128]{2,1,0:T(8,128)(2,1)}), bf16[8,160,128]{2,1,0:T(8,128)(2,1)S(1)}, u32[]{:S(2)}, u32[]{:S(2)}) %all-to-all-start.1) | async-done | bytes 327712 | tf_op jit(solution)/shard_map/all_to_all | solution.py:305
  32.7 29.2 %all-gather.1 = bf16[2304,128]{1,0:T(8,128)(2,1)S(1)} all-gather(bf16[288,128]{1,0:T(8,128)(2,1)S(1)} %shard_map.194), channel_id=3, replica_groups=mesh['far'=8,'pair'=2,'y'=4,'x'=4,'core'=2] {'far'}, dimensions={0}, use_global_device_ids=true | all-gather | bytes 663552 | tf_op jit(solution)/shard_map/all_gather | solution.py:368
  61.9 2.4 %shard_map.195 = bf16[8,272,128]{2,1,0:T(8,128)(2,1)S(1)} custom-call(s32[2]{0:T(128)S(1)} %pad_add_fusion.place_ref, f32[1,1]{1,0:T(1,128)} %bitcast.16.weight_ref, bf16[8,160,128]{2,1,0:T(8,128)(2,1)S(1)} %all-to-all-done.1.team_ref, bf16[8,288,128]{2,1,0:T(8,128)(2,1)S(1)} %bitcast.17), custom_call_target="tpu_custom_call" | custom-call | tf_op jit(solution)/shard_map/pallas_call | solution.py:369
  64.3 0.0 copy-start.5
  64.3 0.0 copy-start.6
  64.3 11.5 %all_to_all.20.parts_ref = bf16[8,272,128]{2,1,0:T(8,128)(2,1)S(1)} all-to-all(bf16[8,272,128]{2,1,0:T(8,128)(2,1)S(1)} %shard_map.195), channel_id=1, replica_groups=mesh['far'=8,'pair'=2,'y'=4,'x'=4,'core'=2] {'pair','y'}, dimensions={0} | all-to-all | bytes 1114112 | tf_op jit(solution)/shard_map/all_to_all | solution.py:305
  75.8 0.0 copy-done.5
  75.8 0.0 copy-done.6
  75.8 1.0 %shard_map.196 = bf16[128,2048]{1,0:T(8,128)(2,1)S(1)} custom-call(bf16[8,272,128]{2,1,0:T(8,128)(2,1)S(1)} %all_to_all.20.parts_ref, f32[128,128]{1,0:T(8,128)S(1)} %get-tuple-element.28.local_ref, bf16[128,64]{1,0:T(8,128)(2,1)S(1)} %get-tuple-element.29.decayed_ref, f32[128,128]{1,0:T(8,128)S(1)} %get-tuple-element.30.gate_ref, ...), custom_call_target="tpu_custom_call" | custom-call | tf_op jit(solution)/shard_map/pallas_call | solution.py:382
  76.8 19.9 %all_to_all.21 = bf16[8,16,2048]{2,1,0:T(8,128)(2,1)S(1)} all-to-all(bf16[8,16,2048]{2,1,0:T(8,128)(2,1)S(1)} %bitcast.19), channel_id=1, replica_groups=mesh['far'=8,'pair'=2,'y'=4,'x'=4,'core'=2] {'x','core'}, dimensions={0} | all-to-all | bytes 1048576 | tf_op jit(solution)/shard_map/all_to_all | solution.py:305
  96.7 0.7 reduce_sum.12
  (1 shorter events, 0.0 us)
Async XLA Ops:
  0.0 0.8 copy-start.10
  0.8 5.8 %copy-start.12 = (bf16[32,64]{1,0:T(8,128)(2,1)S(1)}, bf16[32,64]{1,0:T(8,128)(2,1)}, u32[]{:S(2)}) copy-start(bf16[32,64]{1,0:T(8,128)(2,1)} %up_ref.1) | copy-start | bytes 12292
  0.8 19.6 %copy-start.9 = (bf16[2048,32]{0,1:T(8,128)(2,1)S(1)}, bf16[2048,32]{0,1:T(8,128)(2,1)}, u32[]{:S(2)}) copy-start(bf16[2048,32]{0,1:T(8,128)(2,1)} %param.33) | copy-start | bytes 393220
  1.6 5.0 %copy-start.11 = (f32[2048]{0:T(1024)S(1)}, f32[2048]{0:T(1024)}, u32[]{:S(2)}) copy-start(f32[2048]{0:T(1024)} %param.21) | copy-start | bytes 24580
  1.6 5.0 %copy-start.13 = (f32[64]{0:T(128)S(1)}, f32[64]{0:T(128)}, u32[]{:S(2)}) copy-start(f32[64]{0:T(128)} %param.35) | copy-start | bytes 772
  1.6 5.1 %copy-start.14 = (f32[128,1]{0,1:T(1,128)S(1)}, f32[128,1]{0,1:T(1,128)}, u32[]{:S(2)}) copy-start(f32[128,1]{0,1:T(1,128)} %param.36) | copy-start | bytes 1540
  1.6 5.1 %copy-start.15 = (f32[64]{0:T(128)S(1)}, f32[64]{0:T(128)}, u32[]{:S(2)}) copy-start(f32[64]{0:T(128)} %param.25) | copy-start | bytes 772
  1.6 5.1 %copy-start.16 = (f32[64]{0:T(128)S(1)}, f32[64]{0:T(128)}, u32[]{:S(2)}) copy-start(f32[64]{0:T(128)} %param.26) | copy-start | bytes 772
  1.6 5.1 %copy-start.17 = (f32[128]{0:T(128)S(1)}, f32[128]{0:T(128)}, u32[]{:S(2)}) copy-start(f32[128]{0:T(128)} %param.28) | copy-start | bytes 1540
  1.6 5.1 %copy-start.18 = (f32[128]{0:T(128)S(1)}, f32[128]{0:T(128)}, u32[]{:S(2)}) copy-start(f32[128]{0:T(128)} %param.37) | copy-start | bytes 1540
  1.6 18.9 %copy-start.4 = (bf16[2048,128]{1,0:T(8,128)(2,1)S(1)}, bf16[2048,128]{1,0:T(8,128)(2,1)}, u32[]{:S(2)}) copy-start(bf16[2048,128]{1,0:T(8,128)(2,1)} %lv_ref.1) | copy-start | bytes 1572868
  1.6 10.5 %all-to-all-start = ((bf16[4,16,2048]{2,1,0:T(8,128)(2,1)}), bf16[4,16,2048]{2,1,0:T(8,128)(2,1)S(1)}, u32[]{:S(2)}, u32[]{:S(2)}) async-start(bf16[4,16,2048]{2,1,0:T(8,128)(2,1)} %shard_map.190), calls=%async_computation | async-start | bytes 524288 | tf_op jit(solution)/shard_map/all_to_all | solution.py:305
  6.6 13.9 %copy-start.3 = (bf16[2048,128]{1,0:T(8,128)(2,1)S(1)}, bf16[2048,128]{1,0:T(8,128)(2,1)}, u32[]{:S(2)}) copy-start(bf16[2048,128]{1,0:T(8,128)(2,1)} %dq_ref.1) | copy-start | bytes 1572868
  6.8 13.7 %copy-start.8 = (bf16[2048,64]{0,1:T(8,128)(2,1)S(1)}, bf16[2048,64]{0,1:T(8,128)(2,1)}, u32[]{:S(2)}) copy-start(bf16[2048,64]{0,1:T(8,128)(2,1)} %param.30) | copy-start | bytes 786436
  20.5 6.5 %copy-start.1 = (bf16[2048,128]{1,0:T(8,128)(2,1)S(1)}, bf16[2048,128]{1,0:T(8,128)(2,1)}, u32[]{:S(2)}) copy-start(bf16[2048,128]{1,0:T(8,128)(2,1)} %dv_ref.1) | copy-start | bytes 1572868
  20.5 6.5 %copy-start.2 = (bf16[2048,128]{1,0:T(8,128)(2,1)S(1)}, bf16[2048,128]{1,0:T(8,128)(2,1)}, u32[]{:S(2)}) copy-start(bf16[2048,128]{1,0:T(8,128)(2,1)} %lg_ref.1) | copy-start | bytes 1572868
  20.5 6.5 %copy-start.7 = (bf16[2048,64]{0,1:T(8,128)(2,1)S(1)}, bf16[2048,64]{0,1:T(8,128)(2,1)}, u32[]{:S(2)}) copy-start(bf16[2048,64]{0,1:T(8,128)(2,1)} %param.29) | copy-start | bytes 786436
  22.7 4.3 %copy-start = (bf16[2048,128]{1,0:T(8,128)(2,1)S(1)}, bf16[2048,128]{1,0:T(8,128)(2,1)}, u32[]{:S(2)}) copy-start(bf16[2048,128]{1,0:T(8,128)(2,1)} %dk_ref.1) | copy-start | bytes 1572868
  22.7 10.0 %all-to-all-start.1 = ((bf16[8,160,128]{2,1,0:T(8,128)(2,1)}), bf16[8,160,128]{2,1,0:T(8,128)(2,1)S(1)}, u32[]{:S(2)}, u32[]{:S(2)}) async-start(bf16[8,160,128]{2,1,0:T(8,128)(2,1)} %get-tuple-element.22), calls=%async_computation.1 | async-start | bytes 655360 | tf_op jit(solution)/shard_map/all_to_all | solution.py:305
  64.3 11.5 %copy-start.5 = (bf16[128,2048]{1,0:T(8,128)(2,1)S(1)}, bf16[128,2048]{1,0:T(8,128)(2,1)}, u32[]{:S(2)}) copy-start(bf16[128,2048]{1,0:T(8,128)(2,1)} %drows_ref.1) | copy-start | bytes 1572868
  64.3 11.5 %copy-start.6 = (bf16[128,2048]{1,0:T(8,128)(2,1)S(1)}, bf16[128,2048]{1,0:T(8,128)(2,1)}, u32[]{:S(2)}) copy-start(bf16[128,2048]{1,0:T(8,128)(2,1)} %lrows_ref.1) | copy-start | bytes 1572868

commit v6 on v4

--- a/solution.py
+++ b/solution.py
@@ -88,8 +88,8 @@
     normed = (rows * lax.rsqrt(mean_sq + RMS_EPS) * gain_ref[...]).astype(BF16)
     normed_ref[...] = normed
 
-    lk = dot_nt(normed, lk_ref[...]).astype(BF16)
-    low = dot_nt(normed, down_ref[...]).astype(BF16)
+    narrow = dot_nt(normed, jnp.concatenate([lk_ref[...], down_ref[...]], axis=0)).astype(BF16)
+    lk, low = narrow[:, :HEAD], narrow[:, HEAD:]
     lv = dot(normed, lv_ref[...]).astype(BF16)
     lk_out_ref[...] = lk
     lv_out_ref[...] = lv

time: 97.9 us -> 97.8 us (level)
  no operation moved by 1% of the time
where the time goes in v6:
time: 97.8 us; the launch traced here: 97.4 us
  blocking collectives  69 us (71%)
  waiting for transfers between devices  9.81 us (10%)
  starting transfers between devices  8.54 us (9%)
  Pallas kernels  7.51 us (8%)
    all_to_all x2, blocking collectives, exchanged(): return lax.all_to_all(blocks, axis, split_axis=0, concat_axis=0, tiled=True)  31.5 us
    all_gather x1, blocking collectives, per_device(): far = lax.all_gather(far, 'far')  29.1 us
    all_to_all x2, waiting for transfers between devices, exchanged(): return lax.all_to_all(blocks, axis, split_axis=0, concat_axis=0, tiled=True)  9.81 us
    all_to_all x2, starting transfers between devices, exchanged(): return lax.all_to_all(blocks, axis, split_axis=0, concat_axis=0, tiled=True)  8.54 us
    all_gather x1, blocking collectives, per_device(): rows = lax.all_gather(rows, 'core')  8.33 us
    pallas_call x1, Pallas kernels, per_device(): call(attend_kernel, shape((MEMBERS, 2 * BLOCK + 32, VDIM), BF16), scratch...  2.37 us
    pallas_call x1, Pallas kernels, per_device(): call(project_kernel, (shape((MEMBERS, BLOCK + 32, VDIM), BF16), shape((BL...  2.04 us
  transfers between devices with their start and end apart: 2, of which 2 were waited for; matrix products, arithmetic and copies ran while one was open for 0% of the time, Pallas kernels for 1%

profile of v6, /device:TPU:1, one launch (start us, length us, event | category | flops | bytes accessed | tf_op | source)
XLA Modules:
  0.0 97.4 jit_solution(549010211954003723)
XLA Ops:
  0.0 0.0 copy-start.10
  0.0 0.8 copy-done.10
  0.8 0.0 copy-start.12
  0.8 0.0 copy-start.9
  0.8 0.7 shard_map.190
  1.6 0.0 copy-start.11
  1.6 0.0 copy-start.13
  1.6 0.0 copy-start.14
  1.6 0.0 copy-start.15
  1.6 0.0 copy-start.16
  1.6 0.0 copy-start.17
  1.6 0.0 copy-start.18
  1.6 0.0 copy-start.4
  1.6 5.0 %all-to-all-start = ((bf16[4,16,2048]{2,1,0:T(8,128)(2,1)}), bf16[4,16,2048]{2,1,0:T(8,128)(2,1)S(1)}, u32[]{:S(2)}, u32[]{:S(2)}) async-start(bf16[4,16,2048]{2,1,0:T(8,128)(2,1)} %shard_map.190), calls=%async_computation | async-start | bytes 524288 | tf_op jit(solution)/shard_map/all_to_all | solution.py:306
  6.6 0.0 copy-start.3
  6.6 0.0 copy-done.12
  6.6 0.0 copy-done.11
  6.6 0.0 copy-done.13
  6.6 0.0 copy-done.14
  6.6 0.0 copy-done.15
  6.6 0.0 copy-done.16
  6.6 0.0 copy-done.17
  6.7 0.0 copy-done.18
  6.7 0.1 shard_map.191
  6.8 0.0 copy-start.8
  6.8 5.3 %all-to-all-done = bf16[4,16,2048]{2,1,0:T(8,128)(2,1)S(1)} async-done(((bf16[4,16,2048]{2,1,0:T(8,128)(2,1)}), bf16[4,16,2048]{2,1,0:T(8,128)(2,1)S(1)}, u32[]{:S(2)}, u32[]{:S(2)}) %all-to-all-start) | async-done | bytes 262176 | tf_op jit(solution)/shard_map/all_to_all | solution.py:306
  12.1 8.3 %all-gather = bf16[8,16,2048]{2,1,0:T(8,128)(2,1)S(1)} all-gather(bf16[4,16,2048]{2,1,0:T(8,128)(2,1)S(1)} %all-to-all-done), channel_id=2, replica_groups=mesh['far'=8,'pair'=2,'y'=4,'x'=4,'core'=2] {'core'}, dimensions={0}, use_global_device_ids=true | all-gather | bytes 786432 | tf_op jit(solution)/shard_map/all_gather | solution.py:320
  20.5 0.0 copy-done.9
  20.5 0.0 copy-done.4
  20.5 0.0 copy-done.3
  20.5 0.0 copy-done.8
  20.5 0.0 copy-start.1
  20.5 0.0 copy-start.2
  20.5 0.0 copy-start.7
  20.5 2.0 %shard_map.192 = (bf16[8,160,128]{2,1,0:T(8,128)(2,1)}, bf16[128,2048]{1,0:T(8,128)(2,1)S(1)}, bf16[128,64]{1,0:T(8,128)(2,1)S(1)}, bf16[128,128]{1,0:T(8,128)(2,1)S(1)}, f32[128,64]{1,0:T(8,128)S(1)}) custom-call(bf16[2,4,16,2048]{3,2,1,0:T(8,128)(2,1)S(1)} %bitcast.18, f32[1,2048]{1,0:T(1,128)S(1)} %get-tuple-element.18.gain_ref, ...), custom_call_target="tpu_custom_call" | custom-call | tf_op jit(solution)/shard_map/pallas_call | solution.py:339
  22.5 0.0 copy-start
  22.5 3.6 %all-to-all-start.1 = ((bf16[8,160,128]{2,1,0:T(8,128)(2,1)}), bf16[8,160,128]{2,1,0:T(8,128)(2,1)S(1)}, u32[]{:S(2)}, u32[]{:S(2)}) async-start(bf16[8,160,128]{2,1,0:T(8,128)(2,1)} %get-tuple-element.22), calls=%async_computation.1 | async-start | bytes 655360 | tf_op jit(solution)/shard_map/all_to_all | solution.py:306
  26.8 0.1 pad_add_fusion.place_ref
  26.8 0.0 copy-done.1
  26.9 0.0 copy-done.2
  26.9 0.0 copy-done.7
  26.9 0.0 copy-done
  26.9 1.2 %shard_map.193 = (bf16[256,128]{1,0:T(8,128)(2,1)S(1)}, f32[128,128]{1,0:T(8,128)S(1)}, bf16[128,64]{1,0:T(8,128)(2,1)S(1)}, f32[128,128]{1,0:T(8,128)S(1)}) custom-call(bf16[128,2048]{1,0:T(8,128)(2,1)S(1)} %get-tuple-element.23.normed_ref, bf16[2048,128]{1,0:T(8,128)(2,1)S(1)} %copy-done, bf16[2048,128]{1,0:T(8,128)(2,1)S(1)} %copy-done.1, ...), custom_call_target="tpu_custom_call" | custom-call | tf_op jit(solution)/shard_map/pallas_call | solution.py:353
  28.1 4.5 %all-to-all-done.1.team_ref = bf16[8,160,128]{2,1,0:T(8,128)(2,1)S(1)} async-done(((bf16[8,160,128]{2,1,0:T(8,128)(2,1)}), bf16[8,160,128]{2,1,0:T(8,128)(2,1)S(1)}, u32[]{:S(2)}, u32[]{:S(2)}) %all-to-all-start.1) | async-done | bytes 327712 | tf_op jit(solution)/shard_map/all_to_all | solution.py:306
  32.6 29.1 %all-gather.1 = bf16[2304,128]{1,0:T(8,128)(2,1)S(1)} all-gather(bf16[288,128]{1,0:T(8,128)(2,1)S(1)} %shard_map.194), channel_id=3, replica_groups=mesh['far'=8,'pair'=2,'y'=4,'x'=4,'core'=2] {'far'}, dimensions={0}, use_global_device_ids=true | all-gather | bytes 663552 | tf_op jit(solution)/shard_map/all_gather | solution.py:369
  61.7 2.4 %shard_map.195 = bf16[8,288,128]{2,1,0:T(8,128)(2,1)S(1)} custom-call(s32[2]{0:T(128)S(1)} %pad_add_fusion.place_ref, f32[1,1]{1,0:T(1,128)} %bitcast.16.weight_ref, bf16[8,160,128]{2,1,0:T(8,128)(2,1)S(1)} %all-to-all-done.1.team_ref, bf16[8,288,128]{2,1,0:T(8,128)(2,1)S(1)} %bitcast.17), custom_call_target="tpu_custom_call" | custom-call | tf_op jit(solution)/shard_map/pallas_call | solution.py:370
  64.1 0.0 copy-start.5
  64.1 0.0 copy-start.6
  64.1 12.0 %all_to_all.20.parts_ref = bf16[8,288,128]{2,1,0:T(8,128)(2,1)S(1)} all-to-all(bf16[8,288,128]{2,1,0:T(8,128)(2,1)S(1)} %shard_map.195), channel_id=1, replica_groups=mesh['far'=8,'pair'=2,'y'=4,'x'=4,'core'=2] {'pair','y'}, dimensions={0} | all-to-all | bytes 1179648 | tf_op jit(solution)/shard_map/all_to_all | solution.py:306
  76.1 0.0 copy-done.5
  76.1 0.0 copy-done.6
  76.1 1.0 %shard_map.196 = bf16[128,2048]{1,0:T(8,128)(2,1)S(1)} custom-call(bf16[8,288,128]{2,1,0:T(8,128)(2,1)S(1)} %all_to_all.20.parts_ref, f32[128,128]{1,0:T(8,128)S(1)} %get-tuple-element.28.local_ref, bf16[128,64]{1,0:T(8,128)(2,1)S(1)} %get-tuple-element.29.decayed_ref, f32[128,128]{1,0:T(8,128)S(1)} %get-tuple-element.30.gate_ref, ...), custom_call_target="tpu_custom_call" | custom-call | tf_op jit(solution)/shard_map/pallas_call | solution.py:383
  77.2 19.5 %all_to_all.21 = bf16[8,16,2048]{2,1,0:T(8,128)(2,1)S(1)} all-to-all(bf16[8,16,2048]{2,1,0:T(8,128)(2,1)S(1)} %bitcast.19), channel_id=1, replica_groups=mesh['far'=8,'pair'=2,'y'=4,'x'=4,'core'=2] {'x','core'}, dimensions={0} | all-to-all | bytes 1048576 | tf_op jit(solution)/shard_map/all_to_all | solution.py:306
  96.7 0.7 reduce_sum.12
  (1 shorter events, 0.0 us)
Async XLA Ops:
  0.0 0.8 copy-start.10
  0.8 5.8 %copy-start.12 = (bf16[32,64]{1,0:T(8,128)(2,1)S(1)}, bf16[32,64]{1,0:T(8,128)(2,1)}, u32[]{:S(2)}) copy-start(bf16[32,64]{1,0:T(8,128)(2,1)} %up_ref.1) | copy-start | bytes 12292
  0.8 19.6 %copy-start.9 = (bf16[2048,32]{0,1:T(8,128)(2,1)S(1)}, bf16[2048,32]{0,1:T(8,128)(2,1)}, u32[]{:S(2)}) copy-start(bf16[2048,32]{0,1:T(8,128)(2,1)} %param.33) | copy-start | bytes 393220
  1.6 5.0 %copy-start.11 = (f32[2048]{0:T(1024)S(1)}, f32[2048]{0:T(1024)}, u32[]{:S(2)}) copy-start(f32[2048]{0:T(1024)} %param.21) | copy-start | bytes 24580
  1.6 5.0 %copy-start.13 = (f32[64]{0:T(128)S(1)}, f32[64]{0:T(128)}, u32[]{:S(2)}) copy-start(f32[64]{0:T(128)} %param.35) | copy-start | bytes 772
  1.6 5.1 %copy-start.14 = (f32[128,1]{0,1:T(1,128)S(1)}, f32[128,1]{0,1:T(1,128)}, u32[]{:S(2)}) copy-start(f32[128,1]{0,1:T(1,128)} %param.36) | copy-start | bytes 1540
  1.6 5.1 %copy-start.15 = (f32[64]{0:T(128)S(1)}, f32[64]{0:T(128)}, u32[]{:S(2)}) copy-start(f32[64]{0:T(128)} %param.25) | copy-start | bytes 772
  1.6 5.1 %copy-start.16 = (f32[64]{0:T(128)S(1)}, f32[64]{0:T(128)}, u32[]{:S(2)}) copy-start(f32[64]{0:T(128)} %param.26) | copy-start | bytes 772
  1.6 5.1 %copy-start.17 = (f32[128]{0:T(128)S(1)}, f32[128]{0:T(128)}, u32[]{:S(2)}) copy-start(f32[128]{0:T(128)} %param.28) | copy-start | bytes 1540
  1.6 5.1 %copy-start.18 = (f32[128]{0:T(128)S(1)}, f32[128]{0:T(128)}, u32[]{:S(2)}) copy-start(f32[128]{0:T(128)} %param.37) | copy-start | bytes 1540
  1.6 18.9 %copy-start.4 = (bf16[2048,128]{1,0:T(8,128)(2,1)S(1)}, bf16[2048,128]{1,0:T(8,128)(2,1)}, u32[]{:S(2)}) copy-start(bf16[2048,128]{1,0:T(8,128)(2,1)} %lv_ref.1) | copy-start | bytes 1572868
  1.6 10.5 %all-to-all-start = ((bf16[4,16,2048]{2,1,0:T(8,128)(2,1)}), bf16[4,16,2048]{2,1,0:T(8,128)(2,1)S(1)}, u32[]{:S(2)}, u32[]{:S(2)}) async-start(bf16[4,16,2048]{2,1,0:T(8,128)(2,1)} %shard_map.190), calls=%async_computation | async-start | bytes 524288 | tf_op jit(solution)/shard_map/all_to_all | solution.py:306
  6.6 13.9 %copy-start.3 = (bf16[2048,128]{1,0:T(8,128)(2,1)S(1)}, bf16[2048,128]{1,0:T(8,128)(2,1)}, u32[]{:S(2)}) copy-start(bf16[2048,128]{1,0:T(8,128)(2,1)} %dq_ref.1) | copy-start | bytes 1572868
  6.8 13.7 %copy-start.8 = (bf16[2048,64]{0,1:T(8,128)(2,1)S(1)}, bf16[2048,64]{0,1:T(8,128)(2,1)}, u32[]{:S(2)}) copy-start(bf16[2048,64]{0,1:T(8,128)(2,1)} %param.30) | copy-start | bytes 786436
  20.5 6.4 %copy-start.1 = (bf16[2048,128]{1,0:T(8,128)(2,1)S(1)}, bf16[2048,128]{1,0:T(8,128)(2,1)}, u32[]{:S(2)}) copy-start(bf16[2048,128]{1,0:T(8,128)(2,1)} %dv_ref.1) | copy-start | bytes 1572868
  20.5 6.4 %copy-start.2 = (bf16[2048,128]{1,0:T(8,128)(2,1)S(1)}, bf16[2048,128]{1,0:T(8,128)(2,1)}, u32[]{:S(2)}) copy-start(bf16[2048,128]{1,0:T(8,128)(2,1)} %lg_ref.1) | copy-start | bytes 1572868
  20.5 6.4 %copy-start.7 = (bf16[2048,64]{0,1:T(8,128)(2,1)S(1)}, bf16[2048,64]{0,1:T(8,128)(2,1)}, u32[]{:S(2)}) copy-start(bf16[2048,64]{0,1:T(8,128)(2,1)} %param.29) | copy-start | bytes 786436
  22.5 4.3 %copy-start = (bf16[2048,128]{1,0:T(8,128)(2,1)S(1)}, bf16[2048,128]{1,0:T(8,128)(2,1)}, u32[]{:S(2)}) copy-start(bf16[2048,128]{1,0:T(8,128)(2,1)} %dk_ref.1) | copy-start | bytes 1572868
  22.5 10.0 %all-to-all-start.1 = ((bf16[8,160,128]{2,1,0:T(8,128)(2,1)}), bf16[8,160,128]{2,1,0:T(8,128)(2,1)S(1)}, u32[]{:S(2)}, u32[]{:S(2)}) async-start(bf16[8,160,128]{2,1,0:T(8,128)(2,1)} %get-tuple-element.22), calls=%async_computation.1 | async-start | bytes 655360 | tf_op jit(solution)/shard_map/all_to_all | solution.py:306
  64.1 12.0 %copy-start.5 = (bf16[128,2048]{1,0:T(8,128)(2,1)S(1)}, bf16[128,2048]{1,0:T(8,128)(2,1)}, u32[]{:S(2)}) copy-start(bf16[128,2048]{1,0:T(8,128)(2,1)} %drows_ref.1) | copy-start | bytes 1572868
  64.1 12.0 %copy-start.6 = (bf16[128,2048]{1,0:T(8,128)(2,1)S(1)}, bf16[128,2048]{1,0:T(8,128)(2,1)}, u32[]{:S(2)}) copy-start(bf16[128,2048]{1,0:T(8,128)(2,1)} %lrows_ref.1) | copy-start | bytes 1572868
